TPU v7x, 32 devices: a whole 2x2x4 slice. The times are simulated.
32 devices in a mesh: sp: 16 (over z, y, x), tp: 2 (over core).
Axes of the slice: x: 2, y: 2, z: 4, core: 2. Of those that a mesh axis runs over, the one named last changes fastest.
Arguments:
- tokens: bfloat16 [4096, 2048], P(('sp', 'tp')), may hold values from -6 to 6
- gain: float32 [2048], replicated, may hold values from 0.1 to 1.9
- w_ret_q: bfloat16 [2048, 2048], P(None, 'tp'), may hold values from -0.125 to 0.125
- w_ret_k: bfloat16 [2048, 2048], P(None, 'tp'), may hold values from -0.125 to 0.125
- w_ret_v: bfloat16 [2048, 2048], P(None, 'tp'), may hold values from -0.125 to 0.125
- w_fox_q: bfloat16 [2048, 1024], P(None, 'tp'), may hold values from -0.125 to 0.125
- w_fox_k: bfloat16 [2048, 1024], P(None, 'tp'), may hold values from -0.125 to 0.125
- w_fox_v: bfloat16 [2048, 1024], P(None, 'tp'), may hold values from -0.125 to 0.125
- fox_gates: float32 [4096, 8], P('sp', 'tp'), may hold values from -4096 to 0, as said below
- w_out_ret: bfloat16 [2048, 2048], P('tp', 'sp'), may hold values from -0.109375 to 0.109375
- w_out_fox: bfloat16 [1024, 2048], P('tp', 'sp'), may hold values from -0.109375 to 0.109375
Outputs:
- mixed: bfloat16 [4096, 2048], P(('sp', 'tp'))
Inputs may be any that keep to these rules, and one draw needn't show every extreme that they name: `fox_gates`: each head's values never rise along positions.
All inputs are finite; a program needn't handle non-finite values.
Results may differ from a plain program's by a relative error of at most 0.02.
Values may be sent and summed in bfloat16 or wider, within the bound.
A program may use at most 128 MiB of HBM per device.

v0:
```python
import functools
import math

import jax
import jax.numpy as jnp
from jax import lax
from jax.experimental import pallas as pl
from jax.experimental.pallas import tpu as pltpu
from jax.sharding import PartitionSpec as P

RET_HEADS = 8
RET_DIM = 256
FOX_DIM = 128
BLOCK = 128
MESH = pl.DeviceIdType.MESH
VMEM_LIMIT = 60 * 1024 * 1024

eps = 1e-06


def remote(src, dst, send, recv, sp, tp):
    return pltpu.make_async_remote_copy(
        src_ref=src,
        dst_ref=dst,
        send_sem=send,
        recv_sem=recv,
        device_id=(sp, tp),
        device_id_type=MESH,
    )


def gather_kernel(
    n_sp,
    n_tp,
    group,
    tok_ref,
    gain_ref,
    gates_ref,
    wr_ref,
    wf_ref,
    cos_ref,
    sin_ref,
    w_in,
    rq,
    rk,
    rv,
    fq,
    fkv,
    gall,
    wz,
    own,
    xall,
    w_ret,
    w_fox,
    local_sem,
    in_sem,
    tsend,
    trecv,
    dsend,
    drecv,
    psend,
    precv,
    gsend,
    grecv,
    usend,
    urecv,
    nsend,
    nrecv,
):
    sp = lax.axis_index("sp")
    tp = lax.axis_index("tp")
    g = lax.rem(sp, group)
    z = sp // group
    depth = n_sp // group
    rows = tok_ref.shape[0]
    half = rows // 2
    krows = wr_ref.shape[0]

    barrier = pltpu.get_barrier_semaphore()
    for i in range(1, n_sp):
        pl.semaphore_signal(
            barrier, inc=1, device_id=(lax.rem(sp + i, n_sp), tp), device_id_type=MESH
        )
    for i in range(1, n_tp):
        pl.semaphore_signal(
            barrier, inc=1, device_id=(sp, lax.rem(tp + i, n_tp)), device_id_type=MESH
        )

    loads = []
    for i in range(6):
        cut = w_ret if i < 3 else w_fox
        size = cut.shape[2]
        columns = pl.ds(pl.multiple_of(g * size, 128), size)
        loads.append(
            pltpu.make_async_copy(w_in[i].at[:, columns], cut.at[i % 3], in_sem.at[i])
        )

    values = tok_ref[...].astype(jnp.float32)
    scale = lax.rsqrt(jnp.mean(values * values, axis=1, keepdims=True) + eps)
    own[...] = (values * scale * gain_ref[...]).astype(jnp.bfloat16)
    copies = [
        pltpu.make_async_copy(wr_ref, wz.at[z, pl.ds(0, krows)], local_sem.at[0]),
        pltpu.make_async_copy(
            wf_ref, wz.at[z, pl.ds(krows, wf_ref.shape[0])], local_sem.at[1]
        ),
        pltpu.make_async_copy(gates_ref, gall.at[sp], local_sem.at[2]),
    ]
    for copy in copies + loads:
        copy.start()
    pl.semaphore_wait(barrier, n_sp + n_tp - 2)

    def slot(which, core):
        return xall.at[which * n_tp + core]

    mine = pltpu.make_async_copy(own, slot(g, tp), local_sem.at[3])
    mine.start()

    def peer(other):
        return z * group + other

    hyper = group == 4
    direct = []
    for i in range(1, group):
        if hyper and i == 3:
            continue
        other = lax.bitwise_xor(g, i) if hyper else lax.rem(g + i, group)
        direct.append(
            remote(own, slot(g, tp), tsend.at[i], trecv.at[i], peer(other), tp)
        )
    for copy in direct:
        copy.start()
    pair = []
    for i in range(1, n_tp):
        copy = remote(
            own, slot(g, tp), psend.at[0, i], precv.at[0, i], sp, lax.rem(tp + i, n_tp)
        )
        copy.start()
        pair.append(copy)
    gate_copies = []
    for i in range(1, n_sp):
        copy = remote(
            gates_ref, gall.at[sp], gsend.at[i], grecv.at[i], lax.rem(sp + i, n_sp), tp
        )
        copy.start()
        gate_copies.append(copy)

    copies[0].wait()
    copies[1].wait()

    def up(block):
        return remote(
            wz.at[block],
            wz.at[block],
            usend.at[block],
            urecv.at[block],
            lax.rem(sp + group, n_sp),
            tp,
        )

    def down(block):
        return remote(
            wz.at[block],
            wz.at[block],
            nsend.at[block],
            nrecv.at[block],
            lax.rem(sp + n_sp - group, n_sp),
            tp,
        )

    @pl.when(z < depth - 1)
    def _():
        up(z).start()

    @pl.when(z > 0)
    def _():
        down(z).start()

    ready = {0: pair[:]}

    def forward(which, row):
        ready[row] = []
        for i in range(1, n_tp):
            copy = remote(
                slot(which, tp),
                slot(which, tp),
                psend.at[row, i],
                precv.at[row, i],
                sp,
                lax.rem(tp + i, n_tp),
            )
            copy.start()
            pair.append(copy)
            ready[row].append(copy)

    count = n_tp * rows
    half_head = RET_DIM // 2

    def project(which, row):
        for copy in ready[row]:
            copy.wait_recv()
        x = xall[pl.ds(which * n_tp, n_tp)].reshape(count, xall.shape[2])
        span = pl.ds(pl.multiple_of(which * count, count), count)
        for i in range(6):
            cut = w_ret if i < 3 else w_fox
            y = jnp.dot(x, cut[i % 3], preferred_element_type=jnp.float32)
            y = y.astype(jnp.bfloat16)
            if i < 2:
                cosine = cos_ref[span, :]
                sine = sin_ref[span, :]
            for h in range(rq.shape[0] if i < 3 else fq.shape[0]):
                if i < 2:
                    lo = h * RET_DIM
                    a = y[:, lo : lo + half_head].astype(jnp.float32)
                    b = y[:, lo + half_head : lo + RET_DIM].astype(jnp.float32)
                    to = rq if i == 0 else rk
                    by = 1.0 if i == 0 else RET_DIM ** (-0.5)
                    first = (a * cosine - b * sine) * by
                    second = (a * sine + b * cosine) * by
                    to[h, span, :half_head] = first.astype(jnp.bfloat16)
                    to[h, span, half_head:] = second.astype(jnp.bfloat16)
                elif i == 2:
                    rv[h, span, :] = y[:, h * RET_DIM : (h + 1) * RET_DIM]
                elif i == 3:
                    fq[h, span, :] = y[:, h * FOX_DIM : (h + 1) * FOX_DIM]
                else:
                    fkv[i - 4, h, span, :] = y[:, h * FOX_DIM : (h + 1) * FOX_DIM]

    mine.wait()
    for copy in loads:
        copy.wait()
    if not hyper:
        project(g, 0)

    if hyper:
        relays = []
        for i in (1, 2):
            direct[i - 1].wait_recv()
            source = lax.bitwise_xor(g, i)
            target = lax.bitwise_xor(g, 3 - i)
            part = pl.ds((i - 1) * half, half)
            copy = remote(
                slot(source, tp).at[part],
                slot(source, tp).at[part],
                dsend.at[i],
                drecv.at[i],
                peer(target),
                tp,
            )
            copy.start()
            relays.append(copy)
            forward(source, i)
        project(g, 0)
    else:
        for i in range(1, group):
            direct[i - 1].wait_recv()
            forward(lax.rem(g + group - i, group), i)
            project(lax.rem(g + group - i, group), i)

    def line(step, carry):
        below = z - step
        above = z + step

        @pl.when(below >= 0)
        def _():
            up(below).wait_recv()

            @pl.when(z < depth - 1)
            def _():
                up(below).start()

        @pl.when(above <= depth - 1)
        def _():
            down(above).wait_recv()

            @pl.when(z > 0)
            def _():
                down(above).start()

        return carry

    split = depth // 2 if hyper else depth
    lax.fori_loop(1, split, line, 0)
    if hyper:
        project(lax.bitwise_xor(g, 1), 1)
        for copy in relays:
            copy.wait_recv()
        forward(lax.bitwise_xor(g, 3), 3)
    lax.fori_loop(split, depth - 1, line, 0)
    if hyper:
        project(lax.bitwise_xor(g, 2), 2)
        project(lax.bitwise_xor(g, 3), 3)
    lax.fori_loop(max(split, depth - 1), depth, line, 0)

    def settle(step, carry):
        @pl.when((z < depth - 1) & (step <= z))
        def _():
            up(step).wait_send()

        @pl.when((z > 0) & (step >= z))
        def _():
            down(step).wait_send()

        return carry

    lax.fori_loop(0, depth, settle, 0)
    for copy in direct:
        copy.wait_send()
    if hyper:
        for copy in relays:
            copy.wait_send()
    for copy in gate_copies:
        copy.wait()
    for copy in pair:
        copy.wait_send()
    copies[2].wait()


def gather(
    tokens, gain, gates, w_ret, w_fox, cosine, sine, w_in, hret, hfox, n_sp, n_tp, group
):
    rows, width = tokens.shape
    depth = n_sp // group
    out_rows = w_ret.shape[0] + w_fox.shape[0]
    vmem = pl.BlockSpec(memory_space=pltpu.VMEM)
    hbm = pl.BlockSpec(memory_space=pl.ANY)
    dma = pltpu.SemaphoreType.DMA
    run = rows * n_tp * group
    bf16 = jnp.bfloat16

    def body(*refs):
        gather_kernel(n_sp, n_tp, group, *refs[:7], refs[7:13], *refs[13:])

    return pl.pallas_call(
        body,
        out_shape=(
            jax.ShapeDtypeStruct((hret, run, RET_DIM), bf16),
            jax.ShapeDtypeStruct((hret, run, RET_DIM), bf16),
            jax.ShapeDtypeStruct((hret, run, RET_DIM), bf16),
            jax.ShapeDtypeStruct((hfox, run, FOX_DIM), bf16),
            jax.ShapeDtypeStruct((2, hfox, run, FOX_DIM), bf16),
            jax.ShapeDtypeStruct((n_sp,) + gates.shape, jnp.float32),
            jax.ShapeDtypeStruct((depth, out_rows, w_ret.shape[1]), jnp.bfloat16),
        ),
        in_specs=[vmem, vmem, vmem, hbm, hbm, vmem, vmem] + [hbm] * 6,
        out_specs=(vmem,) * 7,
        scratch_shapes=[
            pltpu.VMEM((rows, width), bf16),
            pltpu.VMEM((group * n_tp, rows, width), bf16),
            pltpu.VMEM((3, width, hret * RET_DIM), bf16),
            pltpu.VMEM((3, width, hfox * FOX_DIM), bf16),
            dma((4,)),
            dma((6,)),
            dma((max(group, 2),)),
            dma((max(group, 2),)),
            dma((3,)),
            dma((3,)),
            dma((group, n_tp)),
            dma((group, n_tp)),
            dma((n_sp,)),
            dma((n_sp,)),
            dma((depth,)),
            dma((depth,)),
            dma((depth,)),
            dma((depth,)),
        ],
        compiler_params=pltpu.CompilerParams(
            collective_id=0, has_side_effects=True, vmem_limit_bytes=VMEM_LIMIT
        ),
        name="gather",
    )(tokens, gain, gates, w_ret, w_fox, cosine, sine, *w_in)


def normalize(values):
    return (
        values * lax.rsqrt(jnp.mean(values * values, axis=1, keepdims=True) + eps)
    ).astype(jnp.bfloat16)


def mixer_kernel(
    n_sp,
    n_tp,
    group,
    rq,
    rk,
    rv,
    fq,
    fkv,
    gq,
    gk,
    within,
    qdec,
    kdec,
    bdec,
    wz,
    out,
    w_all,
    slots,
    raw,
    state,
    state_in,
    state_out,
    numer,
    denom,
    ret_buf,
    fox_buf,
    mixed,
    part,
    got,
    local_sem,
    ksend,
    krecv,
    ssend,
    srecv,
    wsend,
    wrecv,
    dsend,
    drecv,
    asend,
    arecv,
    osend,
    orecv,
):
    sp = lax.axis_index("sp")
    tp = lax.axis_index("tp")
    g = lax.rem(sp, group)
    z = sp // group
    depth = n_sp // group
    hret = rq.shape[0]
    hfox = fq.shape[0]
    run = rq.shape[1]
    tok = run // group
    rows = out.shape[0]
    after = lax.rem(sp + group, n_sp)
    before = lax.rem(sp + n_sp - group, n_sp)
    f32 = jnp.float32

    def peer(other):
        return z * group + other

    barrier = pltpu.get_barrier_semaphore()
    for i in range(1, group):
        pl.semaphore_signal(
            barrier, inc=1, device_id=(peer(lax.rem(g + i, group)), tp), device_id_type=MESH
        )
    for i in range(1, n_tp):
        pl.semaphore_signal(
            barrier, inc=1, device_id=(sp, lax.rem(tp + i, n_tp)), device_id_type=MESH
        )
    if depth > 1:

        @pl.when(z < depth - 1)
        def _():
            pl.semaphore_signal(barrier, inc=1, device_id=(after, tp), device_id_type=MESH)

        @pl.when(z > 0)
        def _():
            pl.semaphore_signal(barrier, inc=1, device_id=(before, tp), device_id_type=MESH)

    ends = (z + depth - 1) // depth + (2 * depth - 2 - z) // depth
    pl.semaphore_wait(barrier, group + n_tp - 2 + ends)

    def first_hop():
        return remote(fkv, slots.at[z], ksend.at[z], krecv.at[z], after, tp)

    def hop(block):
        return remote(
            slots.at[block], slots.at[block], ksend.at[block], krecv.at[block], after, tp
        )

    if depth > 1:

        @pl.when(z < depth - 1)
        def _():
            first_hop().start()

    hyper = group == 4
    mine = pltpu.make_async_copy(wz, w_all.at[g], local_sem.at[0])
    mine.start()
    direct = []
    for i in range(1, group):
        if hyper and i == 3:
            continue
        other = lax.bitwise_xor(g, i) if hyper else lax.rem(g + i, group)
        direct.append(
            remote(wz, w_all.at[g], wsend.at[i], wrecv.at[i], peer(other), tp)
        )
    for copy in direct:
        copy.start()

    def relay(i):
        source = lax.bitwise_xor(g, i)
        target = lax.bitwise_xor(g, 3 - i)
        span = pl.ds((i - 1) * (depth // 2), depth // 2)
        return remote(
            w_all.at[source, span],
            w_all.at[source, span],
            dsend.at[i],
            drecv.at[i],
            peer(target),
            tp,
        )

    for h in range(hret):
        state[h] = jnp.zeros(state.shape[1:], f32)

        def ret_step(b, carry):
            span = pl.ds(pl.multiple_of(b * BLOCK, BLOCK), BLOCK)
            q = rq[h, span, :]
            k = rk[h, span, :]
            v = rv[h, span, :]
            scores = (
                lax.dot_general(q, k, (((1,), (1,)), ((), ())), preferred_element_type=f32)
                * within[h]
            )
            inner = jnp.dot(scores.astype(jnp.bfloat16), v, preferred_element_type=f32)
            held = state[h]
            cross = jnp.dot(q, held.astype(jnp.bfloat16), preferred_element_type=f32)
            raw[h, span, :] = inner + cross * qdec[h, pl.ds(0, BLOCK), :]
            scaled = (k.astype(f32) * kdec[h]).astype(jnp.bfloat16)
            update = lax.dot_general(
                scaled, v, (((0,), (0,)), ((), ())), preferred_element_type=f32
            )
            state[h] = held * bdec[h, 0:1, :] + update
            return carry

        lax.fori_loop(0, run // BLOCK, ret_step, 0)

    def state_hop():
        return remote(state_out, state_in, ssend.at[0], srecv.at[0], after, tp)

    if depth > 1:

        @pl.when(z == 0)
        def _():
            state_out[...] = state[...]
            state_hop().start()

    tile = math.gcd(run, 256)
    inverse = FOX_DIM ** (-0.5)

    def attend(h, t, keys, values, key_gates, diagonal, fresh):
        span = pl.ds(pl.multiple_of(t * tile, tile), tile)
        scores = (
            lax.dot_general(
                fq[h, span, :], keys, (((1,), (1,)), ((), ())), preferred_element_type=f32
            )
            * inverse
        )
        scores = scores + gq[h, span, :] - key_gates
        if diagonal:
            row = lax.broadcasted_iota(jnp.int32, scores.shape, 0)
            col = lax.broadcasted_iota(jnp.int32, scores.shape, 1)
            scores = jnp.where(col <= row, scores, -jnp.inf)
        weights = jnp.exp(scores)
        total = jnp.sum(weights, axis=1, keepdims=True)
        product = jnp.dot(weights.astype(jnp.bfloat16), values, preferred_element_type=f32)
        if fresh:
            numer[h, span, :] = product
            denom[h, span, :] = total
        else:
            numer[h, span, :] += product
            denom[h, span, :] += total

    for h in range(hfox):
        for t in range(run // tile):
            for s in range(t, -1, -1):
                span = pl.ds(s * tile, tile)
                attend(
                    h,
                    t,
                    fkv[0, h, span, :],
                    fkv[1, h, span, :],
                    gk[h, z, :, span],
                    s == t,
                    s == t,
                )

    def carried():
        state_hop().wait_recv()

        @pl.when(z < depth - 1)
        def _():
            for h in range(hret):
                state_out[h] = state_in[h] * bdec[h, 1:2, :] + state[h]
            state_hop().start()

        for h in range(hret):
            held = state_in[h].astype(jnp.bfloat16)

            def cross_step(b, carry):
                span = pl.ds(pl.multiple_of(b * tile, tile), tile)
                cross = jnp.dot(rq[h, span, :], held, preferred_element_type=f32)
                raw[h, span, :] += cross * qdec[h, span, :]
                return carry

            lax.fori_loop(0, run // tile, cross_step, 0)

    def earlier(step, carry):
        @pl.when(step <= z)
        def _():
            block = z - step
            hop(block).wait_recv()

            @pl.when(z < depth - 1)
            def _():
                hop(block).start()

            for h in range(hfox):

                def query_step(t, c):
                    attend(
                        h,
                        t,
                        slots[block, 0, h],
                        slots[block, 1, h],
                        gk[h, block],
                        False,
                        False,
                    )
                    return c

                lax.fori_loop(0, run // tile, query_step, 0)

        return carry

    if depth > 1:
        lax.fori_loop(1, 2, earlier, 0)

        @pl.when(z > 0)
        def _():
            carried()

        if hyper:
            direct[0].wait_recv()
            relay(1).start()
            direct[1].wait_recv()
            relay(2).start()
        lax.fori_loop(2, depth, earlier, 0)
    elif hyper:
        direct[0].wait_recv()
        relay(1).start()
        direct[1].wait_recv()
        relay(2).start()

    rw = hret * RET_DIM
    fw = hfox * FOX_DIM
    for t in range(group):
        span = pl.ds(t * tok, tok)
        for h in range(hret):
            ret_buf[t, :, h * RET_DIM : (h + 1) * RET_DIM] = normalize(raw[h, span, :])
        for h in range(hfox):
            fox_buf[t, :, h * FOX_DIM : (h + 1) * FOX_DIM] = normalize(
                numer[h, span, :] / denom[h, span, :]
            )
    ret_cols = pl.ds(pl.multiple_of(g * rw, 128), rw)
    fox_cols = pl.ds(pl.multiple_of(group * rw + g * fw, 128), fw)
    exchange = []
    for i in range(1, group):
        other = lax.rem(g + i, group)
        for kind, (buf, cols) in enumerate(((ret_buf, ret_cols), (fox_buf, fox_cols))):
            copy = remote(
                buf.at[other],
                mixed.at[:, cols],
                asend.at[kind, i],
                arecv.at[kind, i],
                peer(other),
                tp,
            )
            copy.start()
            exchange.append(copy)
    mixed[:, ret_cols] = ret_buf[g]
    mixed[:, fox_cols] = fox_buf[g]
    for copy in exchange:
        copy.wait_recv()
    mine.wait()
    if hyper:
        relay(1).wait_recv()
        relay(2).wait_recv()
    else:
        for copy in direct:
            copy.wait_recv()

    cols = w_all.shape[3]
    pack = max(1, 128 // cols)
    wide = pack * cols
    for t in range(n_tp):
        left = mixed[t * rows : (t + 1) * rows, :]

        def column(p, carry, left=left, t=t):
            blocks = [
                w_all[lax.rem(p * pack + i, group), (p * pack + i) // group]
                for i in range(pack)
            ]
            right = blocks[0] if pack == 1 else jnp.concatenate(blocks, axis=1)
            product = jnp.dot(left, right, preferred_element_type=f32)
            at = pl.ds(pl.multiple_of(p * wide, wide), wide)
            part[t, :, at] = product.astype(jnp.bfloat16)
            return carry

        lax.fori_loop(0, n_sp // pack, column, 0)
    final = []
    for i in range(1, n_tp):
        other = lax.rem(tp + i, n_tp)
        copy = remote(part.at[other], got.at[i], osend.at[i], orecv.at[i], sp, other)
        copy.start()
        final.append(copy)
    total = part[tp].astype(f32)
    for i in range(1, n_tp):
        final[i - 1].wait_recv()
        total = total + got[i].astype(f32)
    out[...] = total.astype(jnp.bfloat16)

    for copy in final + exchange + direct:
        copy.wait_send()
    if hyper:
        relay(1).wait_send()
        relay(2).wait_send()
    if depth > 1:

        @pl.when(z < depth - 1)
        def _():
            first_hop().wait_send()
            state_hop().wait_send()

            def settle(block, carry):
                @pl.when(block < z)
                def _():
                    hop(block).wait_send()

                return carry

            lax.fori_loop(0, depth, settle, 0)


def mixer(rq, rk, rv, fq, fkv, gq, gk, within, qdec, kdec, bdec, wz, rows, n_sp, n_tp, group):
    depth = n_sp // group
    hret, run, _ = rq.shape
    hfox = fq.shape[0]
    tok = run // group
    out_rows, cols = wz.shape[1:]
    width = n_sp * cols
    vmem = pl.BlockSpec(memory_space=pltpu.VMEM)
    dma = pltpu.SemaphoreType.DMA
    f32 = jnp.float32
    bf16 = jnp.bfloat16
    square = (hret, RET_DIM, RET_DIM)
    return pl.pallas_call(
        functools.partial(mixer_kernel, n_sp, n_tp, group),
        out_shape=jax.ShapeDtypeStruct((rows, width), bf16),
        in_specs=[vmem] * 11 + [pl.BlockSpec(memory_space=pl.ANY)],
        out_specs=vmem,
        scratch_shapes=[
            pltpu.VMEM((group,) + wz.shape, bf16),
            pltpu.VMEM((depth,) + fkv.shape, bf16),
            pltpu.VMEM((hret, run, RET_DIM), f32),
            pltpu.VMEM(square, f32),
            pltpu.VMEM(square, f32),
            pltpu.VMEM(square, f32),
            pltpu.VMEM((hfox, run, FOX_DIM), f32),
            pltpu.VMEM((hfox, run, 1), f32),
            pltpu.VMEM((group, tok, hret * RET_DIM), bf16),
            pltpu.VMEM((group, tok, hfox * FOX_DIM), bf16),
            pltpu.VMEM((tok, out_rows), bf16),
            pltpu.VMEM((n_tp, rows, width), bf16),
            pltpu.VMEM((n_tp, rows, width), bf16),
            dma((1,)),
            dma((depth,)),
            dma((depth,)),
            dma((1,)),
            dma((1,)),
            dma((max(group, 2),)),
            dma((max(group, 2),)),
            dma((3,)),
            dma((3,)),
            dma((2, group)),
            dma((2, group)),
            dma((n_tp,)),
            dma((n_tp,)),
        ],
        compiler_params=pltpu.CompilerParams(
            collective_id=1, has_side_effects=True, vmem_limit_bytes=VMEM_LIMIT
        ),
        name="mixer",
    )(rq, rk, rv, fq, fkv, gq, gk, within, qdec, kdec, bdec, wz)


def decay_rates(head_ids, total):
    heads_float = head_ids.astype(jnp.float32)
    middle = RET_HEADS // 2
    fast_rate = 1.0 / (32.0 + 16.0 * heads_float)
    slow_rate = jnp.exp2(-(heads_float - middle)) / total
    return jnp.where(head_ids < middle, fast_rate, slow_rate)


def per_device(
    n_sp,
    n_tp,
    tokens,
    gain,
    w_ret_q,
    w_ret_k,
    w_ret_v,
    w_fox_q,
    w_fox_k,
    w_fox_v,
    fox_gates,
    w_out_ret,
    w_out_fox,
):
    f32 = jnp.float32
    rows, width = tokens.shape
    ret_heads = w_ret_q.shape[1] // RET_DIM
    fox_heads = w_fox_q.shape[1] // FOX_DIM
    group = math.gcd(math.gcd(ret_heads, fox_heads), n_sp)
    depth = n_sp // group
    hret = ret_heads // group
    hfox = fox_heads // group
    run = rows * n_tp * group
    sp = lax.axis_index("sp")
    g = lax.rem(sp, group)
    z = sp // group

    positions = z * run + jnp.arange(run, dtype=jnp.int32)
    half = RET_DIM // 2
    inverse = 10000.0 ** (-jnp.arange(half, dtype=f32) / half)
    angles = positions.astype(f32)[:, None] * inverse[None, :]
    rq, rk, rv, fq, fkv, gall, wz = gather(
        tokens,
        gain.reshape(1, width),
        fox_gates.T,
        w_out_ret,
        w_out_fox,
        jnp.cos(angles),
        jnp.sin(angles),
        (w_ret_q, w_ret_k, w_ret_v, w_fox_q, w_fox_k, w_fox_v),
        hret,
        hfox,
        n_sp,
        n_tp,
        group,
    )

    head_ids = (
        lax.axis_index("tp") * ret_heads + g * hret + jnp.arange(hret, dtype=jnp.int32)
    )
    rates = decay_rates(head_ids, float(run * depth))
    offsets = jnp.arange(BLOCK, dtype=f32)
    spread = offsets[:, None] - offsets[None, :]
    causal = spread >= 0
    within = jnp.where(
        causal[None], jnp.exp(-rates[:, None, None] * jnp.where(causal, spread, 0.0)[None]), 0.0
    )
    steps = jnp.arange(run, dtype=f32)
    qdec = jnp.exp(-rates[:, None] * (steps[None, :] + 1.0))[:, :, None]
    kdec = jnp.exp(-rates[:, None] * (BLOCK - 1.0 - offsets[None, :]))[:, :, None]
    lengths = jnp.array([BLOCK, run], f32)
    bdec = jnp.broadcast_to(
        jnp.exp(-rates[:, None] * lengths[None, :])[:, :, None], (hret, 2, RET_DIM)
    )

    own_gates = lax.dynamic_slice_in_dim(gall, g * hfox, hfox, 1)
    line = own_gates.transpose(1, 0, 2).reshape(hfox, depth, 1, run)
    gq = lax.dynamic_index_in_dim(line, z, 1, False).reshape(hfox, run, 1)
    return mixer(
        rq, rk, rv, fq, fkv, gq, line, within, qdec, kdec, bdec, wz, rows, n_sp, n_tp, group
    )


def solution(mesh):
    in_specs = (
        P(("sp", "tp"), None),
        P(),
        P(None, "tp"),
        P(None, "tp"),
        P(None, "tp"),
        P(None, "tp"),
        P(None, "tp"),
        P(None, "tp"),
        P("sp", "tp"),
        P("tp", "sp"),
        P("tp", "sp"),
    )
    out_specs = P(("sp", "tp"), None)
    return jax.shard_map(
        functools.partial(per_device, mesh.shape["sp"], mesh.shape["tp"]),
        mesh=mesh,
        in_specs=in_specs,
        out_specs=out_specs,
        check_vma=False,
    )
```

profile of v0, /device:TPU:25, one launch (start us, length us, event | category | flops | bytes accessed | tf_op | source)
XLA Modules:
  0.0 126.2 jit_solution(10052814378817212886)
XLA Ops:
  0.0 3.1 %multiply_sine_fusion = (f32[1024,128]{1,0:T(8,128)}, f32[1024,128]{1,0:T(8,128)}) fusion(f32[128]{0:T(128)S(1)} %multiply_power_fusion, f32[1024]{0:T(1024)S(1)} %add_convert_fusion), kind=kLoop, calls=%fused_computation | loop fusion | flops 131072 | bytes 1053184 | tf_op jit(solution)/shard_map/sin | solution.py:834
  3.1 0.0 copy-start.1
  3.1 38.7 %gather.1 = (bf16[1,1024,256]{2,1,0:T(8,128)(2,1)}, bf16[1,1024,256]{2,1,0:T(8,128)(2,1)}, bf16[1,1024,256]{2,1,0:T(8,128)(2,1)}, bf16[1,1024,128]{2,1,0:T(8,128...) custom-call(bf16[128,2048]{1,0:T(8,128)(2,1)} %refs_0_.1, ...), custom_call_target="tpu_custom_call" | custom-call | tf_op jit(solution)/shard_map/gather/pallas_call | solution.py:333
  41.7 0.9 constant_dynamic-slice_fusion
  42.6 0.0 copy-start
  42.6 1.0 copy.16.gq
  43.8 1.0 multiply_exponential_fusion.qdec
  44.7 0.7 compare_select_fusion.within
  45.4 0.7 multiply_exponential_fusion.1.kdec
  46.1 0.0 copy-done.1
  46.1 0.7 broadcast_in_dim.4.bdec
  46.7 0.0 copy-done
  46.7 77.6 %mixer.1 = bf16[128,2048]{1,0:T(8,128)(2,1)} custom-call(bf16[1,1024,256]{2,1,0:T(8,128)(2,1)} %get-tuple-element.12.rq, bf16[1,1024,256]{2,1,0:T(8,128)(2,1)} %get-tuple-element.13.rk, bf16[1,1024,256]{2,1,0:T(8,128)(2,1)} %get-tuple-element.14.rv, bf16[1,1024,128]{2,1,0:T(8,128)(2,1)} %get-tuple-element.15.fq, ...), custom_call_target="tpu_custom_call" | custom-call | tf_op jit(solution)/shard_map/mixer/pallas_call | solution.py:747
  124.4 1.9 %copy.18 = bf16[128,2048]{1,0:T(8,128)(2,1)} copy(bf16[128,2048]{1,0:T(8,128)(2,1)} %mixer.1) | data formatting | bytes 1048576
  (4 shorter events, 0.0 us)
Async XLA Ops:
  3.1 43.0 %copy-start.1 = (f32[2]{0:T(128)S(1)}, f32[2]{0:T(128)}, u32[]{:S(2)}) copy-start(f32[2]{0:T(128)} %constant.66.clone) | copy-start | bytes 28
  42.6 4.1 %copy-start = (f32[16,1,256]{2,1,0:T(1,128)}, f32[16,1,256]{2,1,0:T(1,128)S(1)}, u32[]{:S(2)}) copy-start(f32[16,1,256]{2,1,0:T(1,128)S(1)} %constant_dynamic-slice_fusion) | copy-start | bytes 49156
where the time goes:
time: 129 us; the launch traced here: 126 us
  Pallas kernels  116 us (90%)
  other arithmetic  5.37 us (4%)
  local copies, waits for them, and re-layouts  4.44 us (3%)
    pallas_call x1, Pallas kernels, mixer(): pl.pallas_call(functools.partial(mixer_kernel, n_sp, n_tp, group), out_sh...  77.6 us
    pallas_call x1, Pallas kernels, gather(): pl.pallas_call(body, out_shape=(jax.ShapeDtypeStruct((hret, run, RET_DIM)...  38.7 us
    sin x1, other arithmetic, per_device(): jnp.sin(angles)  3.05 us

commit v1 on v0

--- a/solution.py
+++ b/solution.py
@@ -784,6 +784,872 @@
     )(rq, rk, rv, fq, fkv, gq, gk, within, qdec, kdec, bdec, wz)
 
 
+def fused_kernel(
+    n_sp,
+    total,
+    tok_ref,
+    gain_ref,
+    gates_ref,
+    inv_ref,
+    wr_ref,
+    wf_ref,
+    w_in,
+    out,
+    xall,
+    w_ret,
+    w_fox,
+    wrs,
+    wret,
+    wfox,
+    gall,
+    ctab,
+    stab,
+    within,
+    qdec,
+    kdec,
+    rq,
+    rk,
+    rv,
+    fq,
+    guest,
+    kv,
+    raw,
+    update,
+    state_in,
+    state_out,
+    carry_state,
+    gcol,
+    guest_col,
+    numer,
+    guest_numer,
+    num_out,
+    num_in,
+    den_out,
+    den_in,
+    part,
+    part_in,
+    rsum,
+    xa,
+    yb,
+    second_out,
+    second_in,
+    fox_buf,
+    mixed,
+    fpart,
+    fgot,
+    local_sem,
+    tsend,
+    trecv,
+    dsend,
+    drecv,
+    psend,
+    precv,
+    gsend,
+    grecv,
+    asend,
+    arecv,
+    usend,
+    urecv,
+    nsend,
+    nrecv,
+    fsend,
+    frecv,
+    ksend,
+    krecv,
+    qsend,
+    qrecv,
+    ssend,
+    srecv,
+    osend,
+    orecv,
+    psum_send,
+    psum_recv,
+    rsend,
+    rrecv,
+    esend,
+    erecv,
+):
+    f32 = jnp.float32
+    bf16 = jnp.bfloat16
+    group = 4
+    sp = lax.axis_index("sp")
+    tp = lax.axis_index("tp")
+    other_core = 1 - tp
+    g = lax.rem(sp, group)
+    z = sp // group
+    depth = n_sp // group
+    last = depth - 1
+    host = depth - 2
+    rows = tok_ref.shape[0]
+    tok = 2 * rows
+    hret = rq.shape[1]
+    hfox = fq.shape[1]
+    ret_rows = hret * RET_DIM
+    after = lax.rem(sp + group, n_sp)
+    before = lax.rem(sp + n_sp - group, n_sp)
+
+    def near(i):
+        return lax.bitwise_xor(g, i)
+
+    def peer(i):
+        return z * group + near(i)
+
+    barrier = pltpu.get_barrier_semaphore()
+    for i in range(1, n_sp):
+        pl.semaphore_signal(
+            barrier, inc=1, device_id=(lax.rem(sp + i, n_sp), tp), device_id_type=MESH
+        )
+    pl.semaphore_signal(barrier, inc=1, device_id=(sp, other_core), device_id_type=MESH)
+
+    locals_ = [
+        pltpu.make_async_copy(wr_ref, wrs, local_sem.at[0]),
+        pltpu.make_async_copy(
+            wr_ref.at[pl.ds(pl.multiple_of(g * ret_rows, ret_rows), ret_rows)],
+            wret.at[z, 0],
+            local_sem.at[1],
+        ),
+        pltpu.make_async_copy(wf_ref, wfox.at[0, z], local_sem.at[2]),
+    ]
+    loads = []
+    for i in range(6):
+        cut = w_ret if i < 3 else w_fox
+        size = cut.shape[2]
+        columns = pl.ds(pl.multiple_of(g * size, 128), size)
+        loads.append(
+            pltpu.make_async_copy(
+                w_in[i].at[:, columns], cut.at[i % 3], local_sem.at[3 + i]
+            )
+        )
+    for copy in locals_ + loads:
+        copy.start()
+
+    values = tok_ref[...].astype(f32)
+    scale = lax.rsqrt(jnp.mean(values * values, axis=1, keepdims=True) + eps)
+    xall[0, tp] = (values * scale * gain_ref[...]).astype(bf16)
+    gall[sp] = gates_ref[...]
+    pl.semaphore_wait(barrier, n_sp)
+
+    def token_copy(i):
+        return remote(xall.at[0, tp], xall.at[i, tp], tsend.at[i], trecv.at[i], peer(i), tp)
+
+    def token_relay(i):
+        span = pl.ds((i - 1) * (rows // 2), rows // 2)
+        return remote(
+            xall.at[i, tp, span],
+            xall.at[3, tp, span],
+            dsend.at[i],
+            drecv.at[i],
+            peer(3 - i),
+            tp,
+        )
+
+    def pair_copy(i):
+        return remote(
+            xall.at[i, tp], xall.at[i, tp], psend.at[i], precv.at[i], sp, other_core
+        )
+
+    def gate_copy(i):
+        return remote(
+            gates_ref, gall.at[sp], gsend.at[i], grecv.at[i], lax.rem(sp + i, n_sp), tp
+        )
+
+    def rows_copy(i):
+        span = pl.ds(pl.multiple_of(near(i) * ret_rows, ret_rows), ret_rows)
+        return remote(wrs.at[span], wret.at[z, i], asend.at[i], arecv.at[i], peer(i), tp)
+
+    def cut_of(kind, block):
+        if kind == 0:
+            return wfox.at[0, block]
+        if kind == 1:
+            return wret.at[block, 0]
+        return wret.at[block, pl.ds(1, group - 1)]
+
+    def up(kind, block):
+        ref = cut_of(kind, block)
+        return remote(ref, ref, usend.at[kind, block], urecv.at[kind, block], after, tp)
+
+    def down(kind, block):
+        ref = cut_of(kind, block)
+        return remote(ref, ref, nsend.at[kind, block], nrecv.at[kind, block], before, tp)
+
+    def begin_line(kind):
+        @pl.when(z < last)
+        def _():
+            up(kind, z).start()
+
+        @pl.when(z > 0)
+        def _():
+            down(kind, z).start()
+
+    def line(kind, step):
+        below = z - step
+        above = z + step
+
+        @pl.when(below >= 0)
+        def _():
+            up(kind, below).wait_recv()
+
+            @pl.when(z < last)
+            def _():
+                up(kind, below).start()
+
+        @pl.when(above <= last)
+        def _():
+            down(kind, above).wait_recv()
+
+            @pl.when(z > 0)
+            def _():
+                down(kind, above).start()
+
+    def settle_line(kind):
+        for block in range(depth):
+
+            @pl.when((z < last) & (block <= z))
+            def _():
+                up(kind, block).wait_send()
+
+            @pl.when((z > 0) & (block >= z))
+            def _():
+                down(kind, block).wait_send()
+
+    def plane_copy(i):
+        return remote(wfox.at[0], wfox.at[i], fsend.at[i], frecv.at[i], peer(i), tp)
+
+    def plane_relay(i):
+        span = pl.ds(0, depth // 2) if i == 1 else pl.ds(depth // 2, depth - depth // 2)
+        return remote(
+            wfox.at[i, span],
+            wfox.at[3, span],
+            fsend.at[2 + i],
+            frecv.at[2 + i],
+            peer(3 - i),
+            tp,
+        )
+
+    def kv_hop(block, i):
+        ref = kv.at[block, i]
+        return remote(ref, ref, ksend.at[block, i], krecv.at[block, i], after, tp)
+
+    def query_hop(i):
+        return remote(fq.at[i], guest.at[i], qsend.at[i], qrecv.at[i], before, tp)
+
+    def state_hop():
+        return remote(state_out, state_in, ssend.at[0], srecv.at[0], after, tp)
+
+    def num_hop(i):
+        return remote(num_out.at[i], num_in.at[i], osend.at[i], orecv.at[i], after, tp)
+
+    def den_hop():
+        return remote(den_out, den_in, osend.at[group], orecv.at[group], after, tp)
+
+    def part_copy(i):
+        return remote(
+            part.at[i, other_core],
+            part_in.at[i],
+            psum_send.at[i],
+            psum_recv.at[i],
+            sp,
+            other_core,
+        )
+
+    width = out.shape[1]
+    half = width // 2
+    first_cols = pl.ds(0, half)
+    last_cols = pl.ds(half, half)
+
+    def scatter_x(k):
+        return remote(
+            rsum.at[1 + 2 * k, :, first_cols],
+            xa.at[k],
+            rsend.at[k],
+            rrecv.at[k],
+            peer(1),
+            tp,
+        )
+
+    def scatter_y(k):
+        return remote(
+            rsum.at[2 + k, :, last_cols],
+            yb.at[k],
+            rsend.at[2 + k],
+            rrecv.at[2 + k],
+            peer(2),
+            tp,
+        )
+
+    def scatter_second(k):
+        return remote(
+            second_out.at[k],
+            second_in.at[k],
+            rsend.at[4 + k],
+            rrecv.at[4 + k],
+            peer(2 if k == 0 else 1),
+            tp,
+        )
+
+    fw = hfox * FOX_DIM
+    my_cols = pl.ds(pl.multiple_of(g * fw, 128), fw)
+
+    def mixed_copy(i):
+        return remote(
+            fox_buf.at[i], mixed.at[:, my_cols], esend.at[i], erecv.at[i], peer(i), tp
+        )
+
+    def final_copy():
+        return remote(
+            fpart.at[other_core], fgot, esend.at[0], erecv.at[0], sp, other_core
+        )
+
+    for i in (1, 2):
+        token_copy(i).start()
+    pair_copy(0).start()
+    for i in range(1, n_sp):
+        gate_copy(i).start()
+    for copy in locals_:
+        copy.wait()
+    for i in range(1, group):
+        rows_copy(i).start()
+    begin_line(0)
+    begin_line(1)
+
+    head_of = [tp * (group * hret) + g * hret + h for h in range(hret)]
+    rates = []
+    for h in range(hret):
+        ids = jnp.full((1, RET_DIM), head_of[h], jnp.int32)
+        heads_float = ids.astype(f32)
+        middle = RET_HEADS // 2
+        fast_rate = 1.0 / (32.0 + 16.0 * heads_float)
+        slow_rate = jnp.exp2(-(heads_float - middle)) / total
+        rates.append(jnp.where(ids < middle, fast_rate, slow_rate))
+    square = (tok, RET_DIM)
+    offset = lax.broadcasted_iota(jnp.int32, square, 0)
+    column = lax.broadcasted_iota(jnp.int32, (tok, tok), 1)
+    row = lax.broadcasted_iota(jnp.int32, (tok, tok), 0)
+    for h in range(hret):
+        rate = rates[h]
+        spread = jnp.maximum(row - column, 0).astype(f32)
+        within[h] = jnp.where(row >= column, jnp.exp(-rate[:, :1] * spread), 0.0)
+        steps = offset.astype(f32)
+        qdec[h] = jnp.exp(-rate * (steps + 1.0))
+        kdec[h] = jnp.exp(-rate * (tok - 1.0 - steps))
+    inverse_freq = inv_ref[...]
+    unit = 16
+    low = lax.broadcasted_iota(jnp.int32, (unit, RET_DIM // 2), 0).astype(f32)
+    high = lax.broadcasted_iota(jnp.int32, (tok // unit, RET_DIM // 2), 0).astype(f32)
+    cos_low, sin_low = jnp.cos(low * inverse_freq), jnp.sin(low * inverse_freq)
+    high = high * float(unit) * inverse_freq
+    cos_high, sin_high = jnp.cos(high), jnp.sin(high)
+    for a in range(tok // unit):
+        ca, sa = cos_high[a : a + 1], sin_high[a : a + 1]
+        ctab[a * unit : (a + 1) * unit] = cos_low * ca - sin_low * sa
+        stab[a * unit : (a + 1) * unit] = sin_low * ca + cos_low * sa
+
+    half_head = RET_DIM // 2
+
+    def retain(i):
+        for h in range(hret):
+            q = rq[i, h]
+            k = rk[i, h]
+            v = rv[i, h]
+            scores = (
+                lax.dot_general(q, k, (((1,), (1,)), ((), ())), preferred_element_type=f32)
+                * within[h]
+            )
+            raw[i, h] = jnp.dot(scores.astype(bf16), v, preferred_element_type=f32)
+            scaled = (k.astype(f32) * kdec[h]).astype(bf16)
+            update[i, h] = lax.dot_general(
+                scaled, v, (((0,), (0,)), ((), ())), preferred_element_type=f32
+            )
+
+    def project(i):
+        x = xall[i].reshape(tok, xall.shape[3])
+        start = jnp.full((1, half_head), z * (group * tok) + near(i) * tok, jnp.int32)
+        turn = start.astype(f32) * inverse_freq
+        cos_turn, sin_turn = jnp.cos(turn), jnp.sin(turn)
+        for m in (4, 5, 3, 1, 2, 0):
+            cut = w_ret if m < 3 else w_fox
+            y = jnp.dot(x, cut[m % 3], preferred_element_type=f32).astype(bf16)
+            if m < 2:
+                cosine = ctab[...] * cos_turn - stab[...] * sin_turn
+                sine = stab[...] * cos_turn + ctab[...] * sin_turn
+            for h in range(hret if m < 3 else hfox):
+                if m < 2:
+                    lo = h * RET_DIM
+                    a = y[:, lo : lo + half_head].astype(f32)
+                    b = y[:, lo + half_head : lo + RET_DIM].astype(f32)
+                    to = rq if m == 0 else rk
+                    by = 1.0 if m == 0 else RET_DIM ** (-0.5)
+                    to[i, h, :, :half_head] = ((a * cosine - b * sine) * by).astype(bf16)
+                    to[i, h, :, half_head:] = ((a * sine + b * cosine) * by).astype(bf16)
+                elif m == 2:
+                    rv[i, h] = y[:, h * RET_DIM : (h + 1) * RET_DIM]
+                elif m == 3:
+                    fq[i, h] = y[:, h * FOX_DIM : (h + 1) * FOX_DIM]
+                else:
+                    kv[z, i, m - 4, h] = y[:, h * FOX_DIM : (h + 1) * FOX_DIM]
+            if m == 5:
+
+                @pl.when(z < last)
+                def _():
+                    kv_hop(z, i).start()
+
+            if m == 3:
+
+                @pl.when(z == last)
+                def _():
+                    query_hop(i).start()
+
+    def take(step, i):
+        block = z - step
+        wanted = block >= 0
+        if step > 1:
+            wanted = wanted & (z < last)
+
+        @pl.when(wanted)
+        def _():
+            kv_hop(block, i).wait_recv()
+
+            @pl.when(z < host)
+            def _():
+                kv_hop(block, i).start()
+
+    for copy in loads:
+        copy.wait()
+    pair_copy(0).wait_recv()
+    project(0)
+    line(0, 1)
+    line(1, 1)
+    take(1, 0)
+    retain(0)
+    for step in range(2, depth):
+        line(0, step)
+        line(1, step)
+    for i in (1, 2):
+        token_copy(i).wait_recv()
+        token_relay(i).start()
+        pair_copy(i).start()
+    for i in range(1, group):
+        rows_copy(i).wait_recv()
+    pair_copy(1).wait_recv()
+    project(1)
+    pair_copy(2).wait_recv()
+    project(2)
+    begin_line(2)
+    for i in (1, 2):
+        plane_copy(i).start()
+    retain(1)
+    retain(2)
+    line(2, 1)
+    take(1, 1)
+    take(1, 2)
+    for i in (1, 2):
+        token_relay(i).wait_recv()
+    pair_copy(3).start()
+    pair_copy(3).wait_recv()
+    project(3)
+    retain(3)
+
+    run_decay = [jnp.exp(-rates[h] * float(group * tok)) for h in range(hret)]
+    tok_decay = [jnp.exp(-rates[h] * float(tok)) for h in range(hret)]
+    for h in range(hret):
+        held = update[g, h]
+        for p in range(1, group):
+            held = held * tok_decay[h] + update[near(p), h]
+        carry_state[h] = held
+
+    @pl.when(z == 0)
+    def _():
+        state_out[...] = carry_state[...].astype(bf16)
+        state_hop().start()
+
+    take(1, 3)
+    for step in range(2, depth):
+        line(2, step)
+
+    @pl.when(z > 0)
+    def _():
+        state_hop().wait_recv()
+
+        @pl.when(z < last)
+        def _():
+            for h in range(hret):
+                state_out[h] = (state_in[h].astype(f32) * run_decay[h] + carry_state[h]).astype(
+                    bf16
+                )
+            state_hop().start()
+
+        carry_state[...] = state_in[...].astype(f32)
+
+    @pl.when(z == 0)
+    def _():
+        carry_state[...] = jnp.zeros(carry_state.shape, f32)
+
+    for i in range(1, n_sp):
+        gate_copy(i).wait_recv()
+
+    def gate_row(plane, i, h):
+        return gall[plane * group + near(i), pl.ds(g * hfox + h, 1), :]
+
+    def spread_columns(line_row, to, i, h):
+        for c in range(tok // 128):
+            piece = line_row[:, c * 128 : (c + 1) * 128]
+            to[i, h, c * 128 : (c + 1) * 128, :] = jnp.broadcast_to(piece, (128, 128)).T
+
+    for h in range(hfox):
+        for i in range(group):
+            spread_columns(gate_row(z, i, h), gcol, i, h)
+
+    @pl.when(z == host)
+    def _():
+        for h in range(hfox):
+            for i in range(group):
+                spread_columns(gate_row(last, i, h), guest_col, i, h)
+
+    inverse = FOX_DIM ** (-0.5)
+
+    def weigh(q, column_gates, keys, key_gates, mask=None):
+        scores = (
+            lax.dot_general(q, keys, (((1,), (1,)), ((), ())), preferred_element_type=f32)
+            * inverse
+        )
+        count = keys.shape[0] // 128
+        scores = scores + jnp.concatenate([column_gates] * count, axis=1) - key_gates
+        if mask is not None:
+            scores = jnp.where(mask, scores, -jnp.inf)
+        return jnp.exp(scores).astype(bf16)
+
+    def widen(v):
+        return jnp.concatenate([v, jnp.ones(v.shape, bf16)], axis=1)
+
+    def own_attention():
+        mask = row >= column
+        for h in range(hfox):
+            for t in range(group):
+                it = near(t)
+                weights, vals = [], []
+                for s in range(t + 1):
+                    js = near(s)
+                    weights.append(
+                        weigh(
+                            fq[it, h],
+                            gcol[it, h],
+                            kv[z, js, 0, h],
+                            gall[z * group + s, pl.ds(g * hfox + h, 1), :],
+                            mask if s == t else None,
+                        )
+                    )
+                    vals.append(kv[z, js, 1, h])
+                w = weights[0] if t == 0 else jnp.concatenate(weights, axis=1)
+                v = vals[0] if t == 0 else jnp.concatenate(vals, axis=0)
+                numer[it, h] = jnp.dot(w, widen(v), preferred_element_type=f32)
+
+    def attend(block, queries, columns, to, fresh, done=None):
+        for h in range(hfox):
+            keys = kv[block, :, 0, h].reshape(group * tok, FOX_DIM)
+            vals = widen(kv[block, :, 1, h].reshape(group * tok, FOX_DIM))
+            key_gates = jnp.concatenate([gate_row(block, i, h) for i in range(group)], axis=1)
+
+            def query_step(j, carry):
+                w = weigh(queries[j, h], columns[j, h], keys, key_gates)
+                product = jnp.dot(w, vals, preferred_element_type=f32)
+                if fresh:
+                    to[j, h] = product
+                else:
+                    to[j, h] += product
+                return carry
+
+            lax.fori_loop(0, group, query_step, 0)
+
+    def hand_back():
+        for i in range(group):
+            for h in range(hfox):
+                num_out[i, h] = guest_numer[i, h, :, :FOX_DIM].astype(bf16)
+                for c in range(tok // 128):
+                    at = (i * hfox + h) * (tok // 128) + c
+                    den = guest_numer[i, h, c * 128 : (c + 1) * 128, FOX_DIM:]
+                    den_out[at : at + 1, :] = den.T[0:1]
+            num_hop(i).start()
+        den_hop().start()
+
+    def take_back():
+        den_hop().wait_recv()
+        for i in range(group):
+            num_hop(i).wait_recv()
+            for h in range(hfox):
+                numer[i, h, :, :FOX_DIM] += num_in[i, h].astype(f32)
+                for c in range(tok // 128):
+                    at = (i * hfox + h) * (tok // 128) + c
+                    den = jnp.broadcast_to(den_in[at : at + 1, :], (128, 128)).T
+                    numer[i, h, c * 128 : (c + 1) * 128, FOX_DIM:] += den
+
+    def earlier(step):
+        wanted = z - step >= 0
+        if step > 1:
+            wanted = wanted & (z < last)
+
+        @pl.when(wanted)
+        def _():
+            block = z - step
+
+            @pl.when(z == host)
+            def _():
+                attend(block, guest, guest_col, guest_numer, step == 1)
+                if step == host:
+                    hand_back()
+
+            attend(block, fq, gcol, numer, False)
+
+    def retention_out():
+        for h in range(hret):
+            held = carry_state[h]
+            for p in range(group):
+                ip = near(p)
+                cross = jnp.dot(rq[ip, h], held.astype(bf16), preferred_element_type=f32)
+                full = raw[ip, h] + cross * qdec[h]
+                rq[ip, h] = normalize(full)
+                if p < group - 1:
+                    held = held * tok_decay[h] + update[ip, h]
+        for i in range(group):
+            left = jnp.concatenate([rq[i, h] for h in range(hret)], axis=1)
+
+            def column_step(p, carry, left=left, i=i):
+                right = jnp.concatenate(
+                    [wret[p // 2, near(2 * lax.rem(p, 2) + e)] for e in range(2)], axis=1
+                )
+                product = jnp.dot(left, right, preferred_element_type=f32).astype(bf16)
+                at = pl.ds(pl.multiple_of(p * 256, 256), 256)
+                part[i, 0, :, at] = product[:rows]
+                part[i, 1, :, at] = product[rows:]
+                return carry
+
+            lax.fori_loop(0, n_sp // 2, column_step, 0)
+            part_copy(i).start()
+
+    own_attention()
+    retention_out()
+    for i in (1, 2):
+        plane_copy(i).wait_recv()
+        plane_relay(i).start()
+
+    @pl.when(z == host)
+    def _():
+        for i in range(group):
+            query_hop(i).wait_recv()
+
+    earlier(1)
+    for i in range(group):
+        part_copy(i).wait_recv()
+        rsum[i] = (part[i, tp].astype(f32) + part_in[i].astype(f32)).astype(bf16)
+    for k in range(2):
+        scatter_x(k).start()
+        scatter_y(k).start()
+    for step in range(2, depth):
+        for i in range(group):
+            take(step, i)
+        earlier(step)
+
+    for k in range(2):
+        scatter_x(k).wait_recv()
+        scatter_y(k).wait_recv()
+    second_out[0] = (rsum[2, :, :half].astype(f32) + xa[1].astype(f32)).astype(bf16)
+    second_out[1] = (rsum[1, :, half:].astype(f32) + yb[1].astype(f32)).astype(bf16)
+    for k in range(2):
+        scatter_second(k).start()
+
+    @pl.when(z == last)
+    def _():
+        take_back()
+
+    for i in range(group):
+        for h in range(hfox):
+            fox_buf[i, :, h * FOX_DIM : (h + 1) * FOX_DIM] = normalize(
+                numer[i, h, :, :FOX_DIM] / numer[i, h, :, FOX_DIM:]
+            )
+        if i > 0:
+            mixed_copy(i).start()
+    mixed[:, my_cols] = fox_buf[0]
+    for i in (1, 2):
+        plane_relay(i).wait_recv()
+    for i in range(1, group):
+        mixed_copy(i).wait_recv()
+
+    def fox_column(p, carry):
+        right = jnp.concatenate(
+            [wfox[near(2 * lax.rem(p, 2) + e), p // 2] for e in range(2)], axis=1
+        )
+        product = jnp.dot(mixed[...], right, preferred_element_type=f32).astype(bf16)
+        at = pl.ds(pl.multiple_of(p * 256, 256), 256)
+        fpart[0, :, at] = product[:rows]
+        fpart[1, :, at] = product[rows:]
+        return carry
+
+    lax.fori_loop(0, n_sp // 2, fox_column, 0)
+    final_copy().start()
+    for k in range(2):
+        scatter_second(k).wait_recv()
+    final_copy().wait_recv()
+    mine = fpart[tp].astype(f32) + fgot[...].astype(f32)
+    ret_low = rsum[0, :, :half].astype(f32) + xa[0].astype(f32) + second_in[0].astype(f32)
+    ret_high = rsum[0, :, half:].astype(f32) + yb[0].astype(f32) + second_in[1].astype(f32)
+    out[:, :half] = (mine[:, :half] + ret_low).astype(bf16)
+    out[:, half:] = (mine[:, half:] + ret_high).astype(bf16)
+
+    for i in (1, 2):
+        token_copy(i).wait_send()
+        token_relay(i).wait_send()
+        plane_copy(i).wait_send()
+        plane_relay(i).wait_send()
+    for i in range(group):
+        pair_copy(i).wait_send()
+        part_copy(i).wait_send()
+    for i in range(1, group):
+        rows_copy(i).wait_send()
+        mixed_copy(i).wait_send()
+    for i in range(1, n_sp):
+        gate_copy(i).wait_send()
+    for kind in range(3):
+        settle_line(kind)
+    for k in range(2):
+        scatter_x(k).wait_send()
+        scatter_y(k).wait_send()
+        scatter_second(k).wait_send()
+    final_copy().wait_send()
+
+    @pl.when(z < last)
+    def _():
+        state_hop().wait_send()
+        for i in range(group):
+            kv_hop(z, i).wait_send()
+
+    for step in range(1, depth):
+
+        @pl.when((z - step >= 0) & (z < host))
+        def _():
+            for i in range(group):
+                kv_hop(z - step, i).wait_send()
+
+    @pl.when(z == last)
+    def _():
+        for i in range(group):
+            query_hop(i).wait_send()
+
+    @pl.when(z == host)
+    def _():
+        for i in range(group):
+            num_hop(i).wait_send()
+        den_hop().wait_send()
+
+
+def fused(tokens, gain, gates, inverse, w_ret, w_fox, w_in, hret, hfox, n_sp):
+    rows, width = tokens.shape
+    group = 4
+    tok = 2 * rows
+    depth = n_sp // group
+    out_cols = n_sp * w_ret.shape[1]
+    half = out_cols // 2
+    ret_rows = hret * RET_DIM
+    fox_rows = group * hfox * FOX_DIM
+    vmem = pl.BlockSpec(memory_space=pltpu.VMEM)
+    hbm = pl.BlockSpec(memory_space=pl.ANY)
+    dma = pltpu.SemaphoreType.DMA
+    f32 = jnp.float32
+    bf16 = jnp.bfloat16
+    square = (hret, RET_DIM, RET_DIM)
+    heads = (group, hfox, tok, FOX_DIM)
+    dens = group * hfox * (tok // 128)
+    total = float(tok * n_sp)
+
+    def body(*refs):
+        fused_kernel(n_sp, total, *refs[:6], refs[6:12], *refs[12:])
+
+    V = pltpu.VMEM
+    return pl.pallas_call(
+        body,
+        out_shape=jax.ShapeDtypeStruct((rows, out_cols), bf16),
+        in_specs=[vmem] * 4 + [hbm] * 8,
+        out_specs=vmem,
+        scratch_shapes=[
+            V((group, 2, rows, width), bf16),
+            V((3, width, ret_rows), bf16),
+            V((3, width, hfox * FOX_DIM), bf16),
+            V(w_ret.shape, bf16),
+            V((depth, group, ret_rows, w_ret.shape[1]), bf16),
+            V((group, depth, fox_rows, w_ret.shape[1]), bf16),
+            V((n_sp,) + gates.shape, f32),
+            V((tok, RET_DIM // 2), f32),
+            V((tok, RET_DIM // 2), f32),
+            V((hret, tok, tok), f32),
+            V((hret, tok, RET_DIM), f32),
+            V((hret, tok, RET_DIM), f32),
+            V((group, hret, tok, RET_DIM), bf16),
+            V((group, hret, tok, RET_DIM), bf16),
+            V((group, hret, tok, RET_DIM), bf16),
+            V(heads, bf16),
+            V(heads, bf16),
+            V((depth, group, 2, hfox, tok, FOX_DIM), bf16),
+            V((group, hret, tok, RET_DIM), f32),
+            V((group,) + square, f32),
+            V(square, bf16),
+            V(square, bf16),
+            V(square, f32),
+            V((group, hfox, tok, 128), f32),
+            V((group, hfox, tok, 128), f32),
+            V((group, hfox, tok, 2 * FOX_DIM), f32),
+            V((group, hfox, tok, 2 * FOX_DIM), f32),
+            V(heads, bf16),
+            V(heads, bf16),
+            V((dens, 128), f32),
+            V((dens, 128), f32),
+            V((group, 2, rows, out_cols), bf16),
+            V((group, rows, out_cols), bf16),
+            V((group, rows, out_cols), bf16),
+            V((2, rows, half), bf16),
+            V((2, rows, half), bf16),
+            V((2, rows, half), bf16),
+            V((2, rows, half), bf16),
+            V((group, tok, hfox * FOX_DIM), bf16),
+            V((tok, fox_rows), bf16),
+            V((2, rows, out_cols), bf16),
+            V((rows, out_cols), bf16),
+            dma((9,)),
+            dma((3,)),
+            dma((3,)),
+            dma((3,)),
+            dma((3,)),
+            dma((group,)),
+            dma((group,)),
+            dma((n_sp,)),
+            dma((n_sp,)),
+            dma((group,)),
+            dma((group,)),
+            dma((3, depth)),
+            dma((3, depth)),
+            dma((3, depth)),
+            dma((3, depth)),
+            dma((5,)),
+            dma((5,)),
+            dma((depth, group)),
+            dma((depth, group)),
+            dma((group,)),
+            dma((group,)),
+            dma((1,)),
+            dma((1,)),
+            dma((group + 1,)),
+            dma((group + 1,)),
+            dma((group,)),
+            dma((group,)),
+            dma((6,)),
+            dma((6,)),
+            dma((group,)),
+            dma((group,)),
+        ],
+        compiler_params=pltpu.CompilerParams(
+            collective_id=2, has_side_effects=True, vmem_limit_bytes=VMEM_LIMIT
+        ),
+        name="fused",
+    )(tokens, gain, gates, inverse, w_ret, w_fox, *w_in)
+
+
 def decay_rates(head_ids, total):
     heads_float = head_ids.astype(jnp.float32)
     middle = RET_HEADS // 2
@@ -816,13 +1682,26 @@
     hret = ret_heads // group
     hfox = fox_heads // group
     run = rows * n_tp * group
+    half = RET_DIM // 2
+    inverse = 10000.0 ** (-jnp.arange(half, dtype=f32) / half)
+    if group == 4 and n_tp == 2 and depth > 2:
+        return fused(
+            tokens,
+            gain.reshape(1, width),
+            fox_gates.T,
+            inverse.reshape(1, half),
+            w_out_ret,
+            w_out_fox,
+            (w_ret_q, w_ret_k, w_ret_v, w_fox_q, w_fox_k, w_fox_v),
+            hret,
+            hfox,
+            n_sp,
+        )
     sp = lax.axis_index("sp")
     g = lax.rem(sp, group)
     z = sp // group
 
     positions = z * run + jnp.arange(run, dtype=jnp.int32)
-    half = RET_DIM // 2
-    inverse = 10000.0 ** (-jnp.arange(half, dtype=f32) / half)
     angles = positions.astype(f32)[:, None] * inverse[None, :]
     rq, rk, rv, fq, fkv, gall, wz = gather(
         tokens,

time: 129 us -> 104 us (0.81); the launches traced: 126 us -> 104 us
  Pallas kernels: 116 us -> 101 us
  other arithmetic: 5.37 us -> 0.52 us
  local copies, waits for them, and re-layouts: 4.44 us -> 1.88 us
    pallas_call x2 -> x1, Pallas kernels: 116 us -> 101 us  [fused(): pl.pallas_call(body, out_shape=jax.ShapeDtypeStruct((rows, out_cols), bf1...]
    sin x1 -> x0, other arithmetic: 3.05 us -> none  [per_device(): jnp.sin(angles)]
    exp x3 -> x0, other arithmetic: 1.64 us -> none  [the longest x1 0.99 us: per_device(): qdec = jnp.exp(-rates[:, None] * (steps[None, :] + 1.0))[:, :, None]]
where the time goes in v1:
time: 104 us
  Pallas kernels  101 us (97%)
  local copies, waits for them, and re-layouts  1.88 us (2%)
    pallas_call x1, Pallas kernels, fused(): pl.pallas_call(body, out_shape=jax.ShapeDtypeStruct((rows, out_cols), bf1...  101 us

profile of v1, /device:TPU:25, one launch (start us, length us, event | category | flops | bytes accessed | tf_op | source)
XLA Modules:
  0.0 103.6 jit_solution(6686214650956335145)
XLA Ops:
  0.0 0.5 multiply_power_fusion.refs_3_
  0.5 101.2 %fused.1 = bf16[128,2048]{1,0:T(8,128)(2,1)} custom-call(bf16[128,2048]{1,0:T(8,128)(2,1)} %refs_0_.1, f32[1,2048]{1,0:T(1,128)} %bitcast.2, f32[4,256]{1,0:T(4,128)} %bitcast.3, f32[1,128]{1,0:T(1,128)} %multiply_power_fusion.refs_3_, bf16[1024,128]{1,0:T(8,128)(2,1)} %refs_4_.1, bf16[512,128]{1,0:T(8,128)(2,1)} %refs_5_.1, bf16[2048,1024]{1,0:T(8,128)(2,1)} %refs_6_.1, ...), custom_call_target="tpu_custom_call" | custom-call | tf_op jit(solution)/shard_map/fused/pallas_call | solution.py:1566
  101.8 1.9 %copy.13 = bf16[128,2048]{1,0:T(8,128)(2,1)} copy(bf16[128,2048]{1,0:T(8,128)(2,1)} %fused.1) | data formatting | bytes 1048576

commit v2 on v1

--- a/solution.py
+++ b/solution.py
@@ -927,7 +927,8 @@
     scale = lax.rsqrt(jnp.mean(values * values, axis=1, keepdims=True) + eps)
     xall[0, tp] = (values * scale * gain_ref[...]).astype(bf16)
     gall[sp] = gates_ref[...]
-    pl.semaphore_wait(barrier, n_sp)
+    with jax.named_scope("barrier"):
+        pl.semaphore_wait(barrier, n_sp)
 
     def token_copy(i):
         return remote(xall.at[0, tp], xall.at[i, tp], tsend.at[i], trecv.at[i], peer(i), tp)
@@ -1054,6 +1055,7 @@
 
     width = out.shape[1]
     half = width // 2
+    wide = width // depth
     first_cols = pl.ds(0, half)
     last_cols = pl.ds(half, half)
 
@@ -1103,14 +1105,15 @@
     for i in (1, 2):
         token_copy(i).start()
     pair_copy(0).start()
-    for i in range(1, n_sp):
-        gate_copy(i).start()
-    for copy in locals_:
-        copy.wait()
-    for i in range(1, group):
-        rows_copy(i).start()
-    begin_line(0)
-    begin_line(1)
+    with jax.named_scope("first_sends"):
+        for i in range(1, n_sp):
+            gate_copy(i).start()
+        for copy in locals_:
+            copy.wait()
+        for i in range(1, group):
+            rows_copy(i).start()
+        begin_line(0)
+        begin_line(1)
 
     head_of = [tp * (group * hret) + g * hret + h for h in range(hret)]
     rates = []
@@ -1146,6 +1149,21 @@
 
     half_head = RET_DIM // 2
 
+    run_decay = [jnp.exp(-rates[h] * float(group * tok)) for h in range(hret)]
+    tok_decay = [jnp.exp(-rates[h] * float(tok)) for h in range(hret)]
+
+    def sum_state():
+        for h in range(hret):
+            held = update[g, h]
+            for p in range(1, group):
+                held = held * tok_decay[h] + update[near(p), h]
+            carry_state[h] = held
+
+        @pl.when(z == 0)
+        def _():
+            state_out[...] = carry_state[...].astype(bf16)
+            state_hop().start()
+
     def retain(i):
         for h in range(hret):
             q = rq[i, h]
@@ -1156,9 +1174,12 @@
                 * within[h]
             )
             raw[i, h] = jnp.dot(scores.astype(bf16), v, preferred_element_type=f32)
-            scaled = (k.astype(f32) * kdec[h]).astype(bf16)
+
+    def gather_state(i):
+        for h in range(hret):
+            scaled = (rk[i, h].astype(f32) * kdec[h]).astype(bf16)
             update[i, h] = lax.dot_general(
-                scaled, v, (((0,), (0,)), ((), ())), preferred_element_type=f32
+                scaled, rv[i, h], (((0,), (0,)), ((), ())), preferred_element_type=f32
             )
 
     def project(i):
@@ -1166,7 +1187,7 @@
         start = jnp.full((1, half_head), z * (group * tok) + near(i) * tok, jnp.int32)
         turn = start.astype(f32) * inverse_freq
         cos_turn, sin_turn = jnp.cos(turn), jnp.sin(turn)
-        for m in (4, 5, 3, 1, 2, 0):
+        for m in (4, 5, 3, 1, 2, 0) if i < 3 else (1, 2, 4, 5, 3, 0):
             cut = w_ret if m < 3 else w_fox
             y = jnp.dot(x, cut[m % 3], preferred_element_type=f32).astype(bf16)
             if m < 2:
@@ -1187,6 +1208,10 @@
                     fq[i, h] = y[:, h * FOX_DIM : (h + 1) * FOX_DIM]
                 else:
                     kv[z, i, m - 4, h] = y[:, h * FOX_DIM : (h + 1) * FOX_DIM]
+            if m == 2:
+                gather_state(i)
+                if i == 3:
+                    sum_state()
             if m == 5:
 
                 @pl.when(z < last)
@@ -1213,79 +1238,54 @@
             def _():
                 kv_hop(block, i).start()
 
-    for copy in loads:
-        copy.wait()
-    pair_copy(0).wait_recv()
-    project(0)
-    line(0, 1)
-    line(1, 1)
-    take(1, 0)
-    retain(0)
-    for step in range(2, depth):
-        line(0, step)
-        line(1, step)
-    for i in (1, 2):
+    def phase(name, *steps):
+        with jax.named_scope(name):
+            for step in steps:
+                step[0](*step[1:])
+
+    def wait_loads():
+        for copy in loads:
+            copy.wait()
+        pair_copy(0).wait_recv()
+
+    def tokens_on(i):
         token_copy(i).wait_recv()
         token_relay(i).start()
         pair_copy(i).start()
-    for i in range(1, group):
-        rows_copy(i).wait_recv()
-    pair_copy(1).wait_recv()
-    project(1)
-    pair_copy(2).wait_recv()
-    project(2)
-    begin_line(2)
-    for i in (1, 2):
-        plane_copy(i).start()
-    retain(1)
-    retain(2)
-    line(2, 1)
-    take(1, 1)
-    take(1, 2)
-    for i in (1, 2):
-        token_relay(i).wait_recv()
-    pair_copy(3).start()
-    pair_copy(3).wait_recv()
-    project(3)
-    retain(3)
-
-    run_decay = [jnp.exp(-rates[h] * float(group * tok)) for h in range(hret)]
-    tok_decay = [jnp.exp(-rates[h] * float(tok)) for h in range(hret)]
-    for h in range(hret):
-        held = update[g, h]
-        for p in range(1, group):
-            held = held * tok_decay[h] + update[near(p), h]
-        carry_state[h] = held
-
-    @pl.when(z == 0)
-    def _():
-        state_out[...] = carry_state[...].astype(bf16)
-        state_hop().start()
-
-    take(1, 3)
-    for step in range(2, depth):
-        line(2, step)
-
-    @pl.when(z > 0)
-    def _():
-        state_hop().wait_recv()
-
-        @pl.when(z < last)
-        def _():
-            for h in range(hret):
-                state_out[h] = (state_in[h].astype(f32) * run_decay[h] + carry_state[h]).astype(
-                    bf16
-                )
-            state_hop().start()
-
-        carry_state[...] = state_in[...].astype(f32)
-
-    @pl.when(z == 0)
-    def _():
-        carry_state[...] = jnp.zeros(carry_state.shape, f32)
-
-    for i in range(1, n_sp):
-        gate_copy(i).wait_recv()
+
+    def wait_rows():
+        for i in range(1, group):
+            rows_copy(i).wait_recv()
+
+    def wait_pair(i):
+        pair_copy(i).wait_recv()
+
+    def tokens_last():
+        for i in (1, 2):
+            token_relay(i).wait_recv()
+        pair_copy(3).start()
+
+    def begin_plane():
+        for i in (1, 2):
+            plane_copy(i).start()
+
+    def pass_state():
+        @pl.when(z > 0)
+        def _():
+            state_hop().wait_recv()
+
+            @pl.when(z < last)
+            def _():
+                for h in range(hret):
+                    held = state_in[h].astype(f32) * run_decay[h] + carry_state[h]
+                    state_out[h] = held.astype(bf16)
+                state_hop().start()
+
+            carry_state[...] = state_in[...].astype(f32)
+
+        @pl.when(z == 0)
+        def _():
+            carry_state[...] = jnp.zeros(carry_state.shape, f32)
 
     def gate_row(plane, i, h):
         return gall[plane * group + near(i), pl.ds(g * hfox + h, 1), :]
@@ -1295,15 +1295,18 @@
             piece = line_row[:, c * 128 : (c + 1) * 128]
             to[i, h, c * 128 : (c + 1) * 128, :] = jnp.broadcast_to(piece, (128, 128)).T
 
-    for h in range(hfox):
-        for i in range(group):
-            spread_columns(gate_row(z, i, h), gcol, i, h)
-
-    @pl.when(z == host)
-    def _():
+    def gate_columns():
+        for i in range(1, n_sp):
+            gate_copy(i).wait_recv()
         for h in range(hfox):
             for i in range(group):
-                spread_columns(gate_row(last, i, h), guest_col, i, h)
+                spread_columns(gate_row(z, i, h), gcol, i, h)
+
+        @pl.when(z == host)
+        def _():
+            for h in range(hfox):
+                for i in range(group):
+                    spread_columns(gate_row(last, i, h), guest_col, i, h)
 
     inverse = FOX_DIM ** (-0.5)
 
@@ -1409,90 +1412,152 @@
                 rq[ip, h] = normalize(full)
                 if p < group - 1:
                     held = held * tok_decay[h] + update[ip, h]
+        for order in ((3, 1), (2, 0)):
+            left = jnp.concatenate(
+                [
+                    jnp.concatenate([rq[i, h] for i in order], axis=0)
+                    for h in range(hret)
+                ],
+                axis=1,
+            )
+
+            def column_step(p, carry, left=left, order=order):
+                right = jnp.concatenate([wret[p, near(e)] for e in range(group)], axis=1)
+                product = jnp.dot(left, right, preferred_element_type=f32).astype(bf16)
+                at = pl.ds(pl.multiple_of(p * wide, wide), wide)
+                for e in range(4):
+                    part[order[e // 2], e % 2, :, at] = product[e * rows : (e + 1) * rows]
+                return carry
+
+            lax.fori_loop(0, depth, column_step, 0)
+            for i in order:
+                part_copy(i).start()
+
+    def plane_on():
+        for i in (1, 2):
+            plane_copy(i).wait_recv()
+            plane_relay(i).start()
+
+    def wait_guest():
+        @pl.when(z == host)
+        def _():
+            for i in range(group):
+                query_hop(i).wait_recv()
+
+    def scatter_first():
+        for i in (3, 1, 2, 0):
+            part_copy(i).wait_recv()
+            rsum[i] = (part[i, tp].astype(f32) + part_in[i].astype(f32)).astype(bf16)
+            if i == 3:
+                scatter_x(1).start()
+                scatter_y(1).start()
+            elif i == 1:
+                scatter_x(0).start()
+            elif i == 2:
+                scatter_y(0).start()
+
+    def scatter_next():
+        for k in range(2):
+            scatter_x(k).wait_recv()
+            scatter_y(k).wait_recv()
+        second_out[0] = (rsum[2, :, :half].astype(f32) + xa[1].astype(f32)).astype(bf16)
+        second_out[1] = (rsum[1, :, half:].astype(f32) + yb[1].astype(f32)).astype(bf16)
+        for k in range(2):
+            scatter_second(k).start()
+
+    def guest_sums():
+        @pl.when(z == last)
+        def _():
+            take_back()
+
+    def send_fox():
         for i in range(group):
-            left = jnp.concatenate([rq[i, h] for h in range(hret)], axis=1)
-
-            def column_step(p, carry, left=left, i=i):
-                right = jnp.concatenate(
-                    [wret[p // 2, near(2 * lax.rem(p, 2) + e)] for e in range(2)], axis=1
+            for h in range(hfox):
+                fox_buf[i, :, h * FOX_DIM : (h + 1) * FOX_DIM] = normalize(
+                    numer[i, h, :, :FOX_DIM] / numer[i, h, :, FOX_DIM:]
                 )
-                product = jnp.dot(left, right, preferred_element_type=f32).astype(bf16)
-                at = pl.ds(pl.multiple_of(p * 256, 256), 256)
-                part[i, 0, :, at] = product[:rows]
-                part[i, 1, :, at] = product[rows:]
-                return carry
-
-            lax.fori_loop(0, n_sp // 2, column_step, 0)
-            part_copy(i).start()
-
-    own_attention()
-    retention_out()
-    for i in (1, 2):
-        plane_copy(i).wait_recv()
-        plane_relay(i).start()
-
-    @pl.when(z == host)
-    def _():
-        for i in range(group):
-            query_hop(i).wait_recv()
-
-    earlier(1)
-    for i in range(group):
-        part_copy(i).wait_recv()
-        rsum[i] = (part[i, tp].astype(f32) + part_in[i].astype(f32)).astype(bf16)
-    for k in range(2):
-        scatter_x(k).start()
-        scatter_y(k).start()
+            if i > 0:
+                mixed_copy(i).start()
+        mixed[:, my_cols] = fox_buf[0]
+
+    def wait_fox():
+        for i in (1, 2):
+            plane_relay(i).wait_recv()
+        for i in range(1, group):
+            mixed_copy(i).wait_recv()
+
+    def fox_out():
+        def fox_column(p, carry):
+            right = jnp.concatenate([wfox[near(e), p] for e in range(group)], axis=1)
+            product = jnp.dot(mixed[...], right, preferred_element_type=f32).astype(bf16)
+            at = pl.ds(pl.multiple_of(p * wide, wide), wide)
+            fpart[0, :, at] = product[:rows]
+            fpart[1, :, at] = product[rows:]
+            return carry
+
+        lax.fori_loop(0, depth, fox_column, 0)
+        final_copy().start()
+
+    def wait_final():
+        for k in range(2):
+            scatter_second(k).wait_recv()
+        final_copy().wait_recv()
+
+    def finish():
+        mine = fpart[tp].astype(f32) + fgot[...].astype(f32)
+        ret_low = rsum[0, :, :half].astype(f32) + xa[0].astype(f32) + second_in[0].astype(f32)
+        ret_high = rsum[0, :, half:].astype(f32) + yb[0].astype(f32) + second_in[1].astype(f32)
+        out[:, :half] = (mine[:, :half] + ret_low).astype(bf16)
+        out[:, half:] = (mine[:, half:] + ret_high).astype(bf16)
+
+    phase("w_loads", (wait_loads,))
+    phase("project0", (project, 0))
+    phase("line01", (line, 0, 1), (line, 1, 1))
+    phase("take10", (take, 1, 0))
+    phase("retain0", (retain, 0))
+    phase("tokens1", (tokens_on, 1))
+    phase("tokens2", (tokens_on, 2))
+    phase("line02", (line, 0, 2), (line, 1, 2))
+    phase("w_pair1", (wait_pair, 1))
+    phase("project1", (project, 1))
+    phase("w_rows", (wait_rows,), (begin_line, 2))
+    phase("w_pair2", (wait_pair, 2))
+    phase("project2", (project, 2))
+    for step in range(3, depth):
+        phase("line0" + str(step), (line, 0, step), (line, 1, step))
+    phase("begin_plane", (begin_plane,))
+    phase("retain1", (retain, 1))
+    phase("line21", (line, 2, 1))
+    phase("tokens3", (tokens_last,))
+    phase("retain2", (retain, 2))
+    phase("w_pair3", (wait_pair, 3))
+    phase("project3", (project, 3))
+    phase("retain3", (retain, 3))
+    phase("gates", (gate_columns,))
+    phase("line22", (line, 2, 2))
+    phase("pass_state", (pass_state,))
+    phase("take11", (take, 1, 1))
+    phase("take12", (take, 1, 2))
+    phase("take13", (take, 1, 3))
+    phase("own_attention", (own_attention,))
+    phase("plane_on", (plane_on,))
+    for step in range(3, depth):
+        phase("line2" + str(step), (line, 2, step))
+    phase("retention_out", (retention_out,))
+    phase("w_guest", (wait_guest,))
+    phase("earlier1", (earlier, 1))
+    phase("scatter1", (scatter_first,))
     for step in range(2, depth):
         for i in range(group):
-            take(step, i)
-        earlier(step)
-
-    for k in range(2):
-        scatter_x(k).wait_recv()
-        scatter_y(k).wait_recv()
-    second_out[0] = (rsum[2, :, :half].astype(f32) + xa[1].astype(f32)).astype(bf16)
-    second_out[1] = (rsum[1, :, half:].astype(f32) + yb[1].astype(f32)).astype(bf16)
-    for k in range(2):
-        scatter_second(k).start()
-
-    @pl.when(z == last)
-    def _():
-        take_back()
-
-    for i in range(group):
-        for h in range(hfox):
-            fox_buf[i, :, h * FOX_DIM : (h + 1) * FOX_DIM] = normalize(
-                numer[i, h, :, :FOX_DIM] / numer[i, h, :, FOX_DIM:]
-            )
-        if i > 0:
-            mixed_copy(i).start()
-    mixed[:, my_cols] = fox_buf[0]
-    for i in (1, 2):
-        plane_relay(i).wait_recv()
-    for i in range(1, group):
-        mixed_copy(i).wait_recv()
-
-    def fox_column(p, carry):
-        right = jnp.concatenate(
-            [wfox[near(2 * lax.rem(p, 2) + e), p // 2] for e in range(2)], axis=1
-        )
-        product = jnp.dot(mixed[...], right, preferred_element_type=f32).astype(bf16)
-        at = pl.ds(pl.multiple_of(p * 256, 256), 256)
-        fpart[0, :, at] = product[:rows]
-        fpart[1, :, at] = product[rows:]
-        return carry
-
-    lax.fori_loop(0, n_sp // 2, fox_column, 0)
-    final_copy().start()
-    for k in range(2):
-        scatter_second(k).wait_recv()
-    final_copy().wait_recv()
-    mine = fpart[tp].astype(f32) + fgot[...].astype(f32)
-    ret_low = rsum[0, :, :half].astype(f32) + xa[0].astype(f32) + second_in[0].astype(f32)
-    ret_high = rsum[0, :, half:].astype(f32) + yb[0].astype(f32) + second_in[1].astype(f32)
-    out[:, :half] = (mine[:, :half] + ret_low).astype(bf16)
-    out[:, half:] = (mine[:, half:] + ret_high).astype(bf16)
+            phase("take" + str(step) + str(i), (take, step, i))
+        phase("earlier" + str(step), (earlier, step))
+    phase("guest_sums", (guest_sums,))
+    phase("send_fox", (send_fox,))
+    phase("scatter2", (scatter_next,))
+    phase("w_fox", (wait_fox,))
+    phase("fox_out", (fox_out,))
+    phase("w_final", (wait_final,))
+    phase("finish", (finish,))
 
     for i in (1, 2):
         token_copy(i).wait_send()

time: 104 us -> 81.1 us (0.78)
  Pallas kernels: 101 us -> 77.7 us
    pallas_call x1, Pallas kernels: 101 us -> 77.7 us  [fused(): pl.pallas_call(body, out_shape=jax.ShapeDtypeStruct((rows, out_cols), bf1...]
where the time goes in v2:
time: 81.1 us; the launch traced here: 80.1 us
  Pallas kernels  77.7 us (96%)
  local copies, waits for them, and re-layouts  1.88 us (2%)
    pallas_call x1, Pallas kernels, fused(): pl.pallas_call(body, out_shape=jax.ShapeDtypeStruct((rows, out_cols), bf1...  77.7 us
    unnamed x1, local copies, waits for them, and re-layouts  1.88 us

profile of v2, /device:TPU:25, one launch (start us, length us, event | category | flops | bytes accessed | tf_op | source)
XLA Modules:
  0.0 80.1 jit_solution(4263792434674071545)
XLA Ops:
  0.0 0.5 multiply_power_fusion.refs_3_
  0.5 77.7 %fused.1 = bf16[128,2048]{1,0:T(8,128)(2,1)} custom-call(bf16[128,2048]{1,0:T(8,128)(2,1)} %refs_0_.1, f32[1,2048]{1,0:T(1,128)} %bitcast.2, f32[4,256]{1,0:T(4,128)} %bitcast.3, f32[1,128]{1,0:T(1,128)} %multiply_power_fusion.refs_3_, bf16[1024,128]{1,0:T(8,128)(2,1)} %refs_4_.1, bf16[512,128]{1,0:T(8,128)(2,1)} %refs_5_.1, bf16[2048,1024]{1,0:T(8,128)(2,1)} %refs_6_.1, ...), custom_call_target="tpu_custom_call" | custom-call | tf_op jit(solution)/shard_map/fused/pallas_call | solution.py:1631
  78.2 1.9 %copy.13 = bf16[128,2048]{1,0:T(8,128)(2,1)} copy(bf16[128,2048]{1,0:T(8,128)(2,1)} %fused.1) | data formatting | bytes 1048576

commit v3 on v2

--- a/solution.py
+++ b/solution.py
@@ -879,7 +879,7 @@
     z = sp // group
     depth = n_sp // group
     last = depth - 1
-    host = depth - 2
+    host = 1
     rows = tok_ref.shape[0]
     tok = 2 * rows
     hret = rq.shape[1]
@@ -982,9 +982,8 @@
         def _():
             down(kind, z).start()
 
-    def line(kind, step):
+    def line_up(kind, step):
         below = z - step
-        above = z + step
 
         @pl.when(below >= 0)
         def _():
@@ -994,6 +993,9 @@
             def _():
                 up(kind, below).start()
 
+    def line_down(kind, step):
+        above = z + step
+
         @pl.when(above <= last)
         def _():
             down(kind, above).wait_recv()
@@ -1001,6 +1003,10 @@
             @pl.when(z > 0)
             def _():
                 down(kind, above).start()
+
+    def line(kind, step):
+        line_up(kind, step)
+        line_down(kind, step)
 
     def settle_line(kind):
         for block in range(depth):
@@ -1031,17 +1037,32 @@
         ref = kv.at[block, i]
         return remote(ref, ref, ksend.at[block, i], krecv.at[block, i], after, tp)
 
-    def query_hop(i):
-        return remote(fq.at[i], guest.at[i], qsend.at[i], qrecv.at[i], before, tp)
-
-    def state_hop():
-        return remote(state_out, state_in, ssend.at[0], srecv.at[0], after, tp)
-
-    def num_hop(i):
-        return remote(num_out.at[i], num_in.at[i], osend.at[i], orecv.at[i], after, tp)
-
-    def den_hop():
-        return remote(den_out, den_in, osend.at[group], orecv.at[group], after, tp)
+    def query_hop(k, i):
+        there = lax.rem(sp + n_sp - (k + 1) * group, n_sp)
+        return remote(fq.at[i], guest.at[k, i], qsend.at[k, i], qrecv.at[k, i], there, tp)
+
+    slices = 4
+    slice_rows = RET_DIM // slices
+
+    def state_hop(c):
+        span = pl.ds(c * slice_rows, slice_rows)
+        return remote(
+            state_out.at[:, span], state_in.at[:, span], ssend.at[c], srecv.at[c], after, tp
+        )
+
+    guests = depth - 1 - host
+
+    def num_hop(k, i):
+        there = lax.rem(sp + (k + 1) * group, n_sp)
+        return remote(
+            num_out.at[k, i], num_in.at[i], osend.at[k, i], orecv.at[i], there, tp
+        )
+
+    def den_hop(k):
+        there = lax.rem(sp + (k + 1) * group, n_sp)
+        return remote(
+            den_out.at[k], den_in, osend.at[k, group], orecv.at[group], there, tp
+        )
 
     def part_copy(i):
         return remote(
@@ -1162,7 +1183,8 @@
         @pl.when(z == 0)
         def _():
             state_out[...] = carry_state[...].astype(bf16)
-            state_hop().start()
+            for c in range(slices):
+                state_hop(c).start()
 
     def retain(i):
         for h in range(hret):
@@ -1181,6 +1203,12 @@
             update[i, h] = lax.dot_general(
                 scaled, rv[i, h], (((0,), (0,)), ((), ())), preferred_element_type=f32
             )
+
+    def queries_of(k):
+        @pl.when(z == host + 1 + k)
+        def _():
+            for i in range(1, group):
+                query_hop(k, i).start()
 
     def project(i):
         x = xall[i].reshape(tok, xall.shape[3])
@@ -1213,30 +1241,35 @@
                 if i == 3:
                     sum_state()
             if m == 5:
-
-                @pl.when(z < last)
+                ready = z < (last, 0, 1, 1)[i]
+
+                @pl.when(ready)
                 def _():
                     kv_hop(z, i).start()
 
-            if m == 3:
-
-                @pl.when(z == last)
-                def _():
-                    query_hop(i).start()
-
-    def take(step, i):
-        block = z - step
-        wanted = block >= 0
-        if step > 1:
-            wanted = wanted & (z < last)
-
-        @pl.when(wanted)
-        def _():
-            kv_hop(block, i).wait_recv()
-
-            @pl.when(z < host)
+            if m == 3 and i == 0:
+                for k in range(guests):
+
+                    @pl.when(z == host + 1 + k)
+                    def _(k=k):
+                        query_hop(k, 0).start()
+
+    def second_piece():
+        @pl.when(z < last - 1)
+        def _():
+            kv_hop(z, 1).start()
+
+    def late_pieces():
+        @pl.when(z < last)
+        def _():
+            for c in range(slices):
+                state_hop(c).wait_send()
+
+        for i in range(1, group):
+
+            @pl.when((z >= (last - 1 if i == 1 else 1)) & (z < last))
             def _():
-                kv_hop(block, i).start()
+                kv_hop(z, i).start()
 
     def phase(name, *steps):
         with jax.named_scope(name):
@@ -1272,14 +1305,16 @@
     def pass_state():
         @pl.when(z > 0)
         def _():
-            state_hop().wait_recv()
-
-            @pl.when(z < last)
-            def _():
-                for h in range(hret):
-                    held = state_in[h].astype(f32) * run_decay[h] + carry_state[h]
-                    state_out[h] = held.astype(bf16)
-                state_hop().start()
+            for c in range(slices):
+                span = slice(c * slice_rows, (c + 1) * slice_rows)
+                state_hop(c).wait_recv()
+
+                @pl.when(z < last)
+                def _():
+                    for h in range(hret):
+                        held = state_in[h, span].astype(f32) * run_decay[h] + carry_state[h, span]
+                        state_out[h, span] = held.astype(bf16)
+                    state_hop(c).start()
 
             carry_state[...] = state_in[...].astype(f32)
 
@@ -1304,9 +1339,10 @@
 
         @pl.when(z == host)
         def _():
-            for h in range(hfox):
-                for i in range(group):
-                    spread_columns(gate_row(last, i, h), guest_col, i, h)
+            for k in range(guests):
+                for h in range(hfox):
+                    for i in range(group):
+                        spread_columns(gate_row(host + 1 + k, i, h), guest_col.at[k], i, h)
 
     inverse = FOX_DIM ** (-0.5)
 
@@ -1352,55 +1388,63 @@
             vals = widen(kv[block, :, 1, h].reshape(group * tok, FOX_DIM))
             key_gates = jnp.concatenate([gate_row(block, i, h) for i in range(group)], axis=1)
 
-            def query_step(j, carry):
-                w = weigh(queries[j, h], columns[j, h], keys, key_gates)
-                product = jnp.dot(w, vals, preferred_element_type=f32)
-                if fresh:
-                    to[j, h] = product
-                else:
-                    to[j, h] += product
+            def query_step(p, carry):
+                for j in (2 * p, 2 * p + 1):
+                    w = weigh(queries[j, h], columns[j, h], keys, key_gates)
+                    product = jnp.dot(w, vals, preferred_element_type=f32)
+                    if fresh:
+                        to[j, h] = product
+                    else:
+                        to[j, h] += product
+                if done is not None and h == hfox - 1:
+                    done(2 * p)
+                    done(2 * p + 1)
                 return carry
 
-            lax.fori_loop(0, group, query_step, 0)
-
-    def hand_back():
+            lax.fori_loop(0, group // 2, query_step, 0)
+
+    lines = tok // 128
+
+    def serve(k):
+        def hand_back(j):
+            for h in range(hfox):
+                num_out[k, j, h] = guest_numer[k, j, h, :, :FOX_DIM].astype(bf16)
+                for c in range(lines):
+                    at = (j * hfox + h) * lines + c
+                    den = guest_numer[k, j, h, c * 128 : (c + 1) * 128, FOX_DIM:]
+                    den_out[k, pl.ds(at, 1), :] = den.T[0:1]
+            num_hop(k, j).start()
+
+        @pl.when(z == host)
+        def _():
+            for i in range(group):
+                query_hop(k, i).wait_recv()
+            for block in range(k + 1):
+                attend(
+                    block,
+                    guest.at[k],
+                    guest_col.at[k],
+                    guest_numer.at[k],
+                    block == 0,
+                    hand_back if block == k else None,
+                )
+            den_hop(k).start()
+
+    def take_back():
+        den_hop(0).wait_recv()
         for i in range(group):
-            for h in range(hfox):
-                num_out[i, h] = guest_numer[i, h, :, :FOX_DIM].astype(bf16)
-                for c in range(tok // 128):
-                    at = (i * hfox + h) * (tok // 128) + c
-                    den = guest_numer[i, h, c * 128 : (c + 1) * 128, FOX_DIM:]
-                    den_out[at : at + 1, :] = den.T[0:1]
-            num_hop(i).start()
-        den_hop().start()
-
-    def take_back():
-        den_hop().wait_recv()
-        for i in range(group):
-            num_hop(i).wait_recv()
+            num_hop(0, i).wait_recv()
             for h in range(hfox):
                 numer[i, h, :, :FOX_DIM] += num_in[i, h].astype(f32)
-                for c in range(tok // 128):
-                    at = (i * hfox + h) * (tok // 128) + c
+                for c in range(lines):
+                    at = (i * hfox + h) * lines + c
                     den = jnp.broadcast_to(den_in[at : at + 1, :], (128, 128)).T
                     numer[i, h, c * 128 : (c + 1) * 128, FOX_DIM:] += den
 
-    def earlier(step):
-        wanted = z - step >= 0
-        if step > 1:
-            wanted = wanted & (z < last)
-
-        @pl.when(wanted)
-        def _():
-            block = z - step
-
-            @pl.when(z == host)
-            def _():
-                attend(block, guest, guest_col, guest_numer, step == 1)
-                if step == host:
-                    hand_back()
-
-            attend(block, fq, gcol, numer, False)
+    def earlier():
+        @pl.when(z > 0)
+        def _():
+            attend(z - 1, fq, gcol, numer, False)
 
     def retention_out():
         for h in range(hret):
@@ -1412,40 +1456,49 @@
                 rq[ip, h] = normalize(full)
                 if p < group - 1:
                     held = held * tok_decay[h] + update[ip, h]
-        for order in ((3, 1), (2, 0)):
-            left = jnp.concatenate(
-                [
-                    jnp.concatenate([rq[i, h] for i in order], axis=0)
-                    for h in range(hret)
-                ],
-                axis=1,
-            )
-
-            def column_step(p, carry, left=left, order=order):
-                right = jnp.concatenate([wret[p, near(e)] for e in range(group)], axis=1)
-                product = jnp.dot(left, right, preferred_element_type=f32).astype(bf16)
-                at = pl.ds(pl.multiple_of(p * wide, wide), wide)
-                for e in range(4):
-                    part[order[e // 2], e % 2, :, at] = product[e * rows : (e + 1) * rows]
-                return carry
-
-            lax.fori_loop(0, depth, column_step, 0)
-            for i in order:
-                part_copy(i).start()
+
+    def ret_product(*order):
+        left = jnp.concatenate(
+            [jnp.concatenate([rq[i, h] for i in order], axis=0) for h in range(hret)], axis=1
+        )
+
+        def column_step(p, carry):
+            right = jnp.concatenate([wret[p, near(e)] for e in range(group)], axis=1)
+            product = jnp.dot(left, right, preferred_element_type=f32).astype(bf16)
+            at = pl.ds(pl.multiple_of(p * wide, wide), wide)
+            for e in range(2 * len(order)):
+                part[order[e // 2], e % 2, :, at] = product[e * rows : (e + 1) * rows]
+            return carry
+
+        lax.fori_loop(0, depth, column_step, 0)
+        for i in order:
+            part_copy(i).start()
 
     def plane_on():
         for i in (1, 2):
             plane_copy(i).wait_recv()
             plane_relay(i).start()
 
-    def wait_guest():
+    def take_all():
+        @pl.when((z > 0) & (z != host))
+        def _():
+            for i in range(group):
+                kv_hop(z - 1, i).wait_recv()
+
+    def serve_first():
         @pl.when(z == host)
         def _():
             for i in range(group):
-                query_hop(i).wait_recv()
-
-    def scatter_first():
-        for i in (3, 1, 2, 0):
+                kv_hop(z - 1, i).wait_recv()
+
+        serve(0)
+
+    def serve_rest():
+        for k in range(1, guests):
+            serve(k)
+
+    def scatter_first(*order):
+        for i in order:
             part_copy(i).wait_recv()
             rsum[i] = (part[i, tp].astype(f32) + part_in[i].astype(f32)).astype(bf16)
             if i == 3:
@@ -1457,16 +1510,15 @@
                 scatter_y(0).start()
 
     def scatter_next():
-        for k in range(2):
-            scatter_x(k).wait_recv()
-            scatter_y(k).wait_recv()
+        scatter_x(1).wait_recv()
+        scatter_y(1).wait_recv()
         second_out[0] = (rsum[2, :, :half].astype(f32) + xa[1].astype(f32)).astype(bf16)
         second_out[1] = (rsum[1, :, half:].astype(f32) + yb[1].astype(f32)).astype(bf16)
         for k in range(2):
             scatter_second(k).start()
 
     def guest_sums():
-        @pl.when(z == last)
+        @pl.when(z > host)
         def _():
             take_back()
 
@@ -1499,6 +1551,8 @@
         final_copy().start()
 
     def wait_final():
+        scatter_x(0).wait_recv()
+        scatter_y(0).wait_recv()
         for k in range(2):
             scatter_second(k).wait_recv()
         final_copy().wait_recv()
@@ -1513,44 +1567,64 @@
     phase("w_loads", (wait_loads,))
     phase("project0", (project, 0))
     phase("line01", (line, 0, 1), (line, 1, 1))
-    phase("take10", (take, 1, 0))
     phase("retain0", (retain, 0))
     phase("tokens1", (tokens_on, 1))
     phase("tokens2", (tokens_on, 2))
     phase("line02", (line, 0, 2), (line, 1, 2))
     phase("w_pair1", (wait_pair, 1))
     phase("project1", (project, 1))
-    phase("w_rows", (wait_rows,), (begin_line, 2))
+    phase("w_rows", (wait_rows,), (begin_line, 2), (second_piece,))
     phase("w_pair2", (wait_pair, 2))
     phase("project2", (project, 2))
     for step in range(3, depth):
         phase("line0" + str(step), (line, 0, step), (line, 1, step))
     phase("begin_plane", (begin_plane,))
     phase("retain1", (retain, 1))
-    phase("line21", (line, 2, 1))
+    phase("retain2", (retain, 2))
     phase("tokens3", (tokens_last,))
-    phase("retain2", (retain, 2))
     phase("w_pair3", (wait_pair, 3))
+    phase("up21", (line_up, 2, 1))
+    phase("down21", (line_down, 2, 1))
     phase("project3", (project, 3))
-    phase("retain3", (retain, 3))
-    phase("gates", (gate_columns,))
-    phase("line22", (line, 2, 2))
+    upper = z > host
+
+    @pl.when(upper)
+    def _():
+        phase("retain3", (retain, 3))
+        phase("gates", (gate_columns,))
+        phase("query0", (queries_of, 0))
+        phase("up22", (line_up, 2, 2))
+
+    @pl.when(z == last)
+    def _():
+        phase("plane_on", (plane_on,), (queries_of, 1))
+
     phase("pass_state", (pass_state,))
-    phase("take11", (take, 1, 1))
-    phase("take12", (take, 1, 2))
-    phase("take13", (take, 1, 3))
+
+    @pl.when(upper & (z < last))
+    def _():
+        phase("plane_on", (plane_on,))
+
+    @pl.when(z <= host)
+    def _():
+        phase("down22", (line_down, 2, 2))
+        phase("retain3", (retain, 3))
+        phase("gates", (gate_columns,))
+        phase("plane_on", (plane_on,))
+
     phase("own_attention", (own_attention,))
-    phase("plane_on", (plane_on,))
     for step in range(3, depth):
         phase("line2" + str(step), (line, 2, step))
+    phase("late_pieces", (late_pieces,))
     phase("retention_out", (retention_out,))
-    phase("w_guest", (wait_guest,))
-    phase("earlier1", (earlier, 1))
-    phase("scatter1", (scatter_first,))
-    for step in range(2, depth):
-        for i in range(group):
-            phase("take" + str(step) + str(i), (take, step, i))
-        phase("earlier" + str(step), (earlier, step))
+    phase("ret_product1", (ret_product, 3, 1))
+    phase("ret_product2", (ret_product, 2, 0))
+    phase("serve0", (serve_first,))
+    phase("scatter1a", (scatter_first, 3, 1))
+    phase("scatter1b", (scatter_first, 2, 0))
+    phase("serve1", (serve_rest,))
+    phase("takes", (take_all,))
+    phase("earlier", (earlier,))
     phase("guest_sums", (guest_sums,))
     phase("send_fox", (send_fox,))
     phase("scatter2", (scatter_next,))
@@ -1559,50 +1633,48 @@
     phase("w_final", (wait_final,))
     phase("finish", (finish,))
 
-    for i in (1, 2):
-        token_copy(i).wait_send()
-        token_relay(i).wait_send()
-        plane_copy(i).wait_send()
-        plane_relay(i).wait_send()
-    for i in range(group):
-        pair_copy(i).wait_send()
-        part_copy(i).wait_send()
-    for i in range(1, group):
-        rows_copy(i).wait_send()
-        mixed_copy(i).wait_send()
-    for i in range(1, n_sp):
-        gate_copy(i).wait_send()
-    for kind in range(3):
-        settle_line(kind)
-    for k in range(2):
-        scatter_x(k).wait_send()
-        scatter_y(k).wait_send()
-        scatter_second(k).wait_send()
-    final_copy().wait_send()
-
-    @pl.when(z < last)
-    def _():
-        state_hop().wait_send()
+    def settle_all():
+        for i in (1, 2):
+            token_copy(i).wait_send()
+            token_relay(i).wait_send()
+            plane_copy(i).wait_send()
+            plane_relay(i).wait_send()
         for i in range(group):
-            kv_hop(z, i).wait_send()
-
-    for step in range(1, depth):
-
-        @pl.when((z - step >= 0) & (z < host))
+            pair_copy(i).wait_send()
+            part_copy(i).wait_send()
+        for i in range(1, group):
+            rows_copy(i).wait_send()
+            mixed_copy(i).wait_send()
+        for i in range(1, n_sp):
+            gate_copy(i).wait_send()
+        for kind in range(3):
+            settle_line(kind)
+        for k in range(2):
+            scatter_x(k).wait_send()
+            scatter_y(k).wait_send()
+            scatter_second(k).wait_send()
+        final_copy().wait_send()
+
+        @pl.when(z < last)
         def _():
             for i in range(group):
-                kv_hop(z - step, i).wait_send()
-
-    @pl.when(z == last)
-    def _():
-        for i in range(group):
-            query_hop(i).wait_send()
-
-    @pl.when(z == host)
-    def _():
-        for i in range(group):
-            num_hop(i).wait_send()
-        den_hop().wait_send()
+                kv_hop(z, i).wait_send()
+
+        for k in range(guests):
+
+            @pl.when(z == host + 1 + k)
+            def _(k=k):
+                for i in range(group):
+                    query_hop(k, i).wait_send()
+
+        @pl.when(z == host)
+        def _():
+            for k in range(guests):
+                for i in range(group):
+                    num_hop(k, i).wait_send()
+                den_hop(k).wait_send()
+
+    phase("settle", (settle_all,))
 
 
 def fused(tokens, gain, gates, inverse, w_ret, w_fox, w_in, hret, hfox, n_sp):
@@ -1622,6 +1694,7 @@
     square = (hret, RET_DIM, RET_DIM)
     heads = (group, hfox, tok, FOX_DIM)
     dens = group * hfox * (tok // 128)
+    guests = depth - 2
     total = float(tok * n_sp)
 
     def body(*refs):
@@ -1650,7 +1723,7 @@
             V((group, hret, tok, RET_DIM), bf16),
             V((group, hret, tok, RET_DIM), bf16),
             V(heads, bf16),
-            V(heads, bf16),
+            V((guests,) + heads, bf16),
             V((depth, group, 2, hfox, tok, FOX_DIM), bf16),
             V((group, hret, tok, RET_DIM), f32),
             V((group,) + square, f32),
@@ -1658,12 +1731,12 @@
             V(square, bf16),
             V(square, f32),
             V((group, hfox, tok, 128), f32),
-            V((group, hfox, tok, 128), f32),
+            V((guests, group, hfox, tok, 128), f32),
             V((group, hfox, tok, 2 * FOX_DIM), f32),
-            V((group, hfox, tok, 2 * FOX_DIM), f32),
+            V((guests, group, hfox, tok, 2 * FOX_DIM), f32),
+            V((guests,) + heads, bf16),
             V(heads, bf16),
-            V(heads, bf16),
-            V((dens, 128), f32),
+            V((guests, dens, 128), f32),
             V((dens, 128), f32),
             V((group, 2, rows, out_cols), bf16),
             V((group, rows, out_cols), bf16),
@@ -1695,11 +1768,11 @@
             dma((5,)),
             dma((depth, group)),
             dma((depth, group)),
-            dma((group,)),
-            dma((group,)),
-            dma((1,)),
-            dma((1,)),
-            dma((group + 1,)),
+            dma((guests, group)),
+            dma((guests, group)),
+            dma((4,)),
+            dma((4,)),
+            dma((guests, group + 1)),
             dma((group + 1,)),
             dma((group,)),
             dma((group,)),
@@ -1749,7 +1822,7 @@
     run = rows * n_tp * group
     half = RET_DIM // 2
     inverse = 10000.0 ** (-jnp.arange(half, dtype=f32) / half)
-    if group == 4 and n_tp == 2 and depth > 2:
+    if group == 4 and n_tp == 2 and depth == 4:
         return fused(
             tokens,
             gain.reshape(1, width),

time: 81.1 us -> 77.8 us (0.959)
  Pallas kernels: 77.7 us -> 74.9 us
    pallas_call x1, Pallas kernels: 77.7 us -> 74.9 us  [fused(): pl.pallas_call(body, out_shape=jax.ShapeDtypeStruct((rows, out_cols), bf1...]
where the time goes in v3:
time: 77.8 us; the launch traced here: 77.3 us
  Pallas kernels  74.9 us (96%)
  local copies, waits for them, and re-layouts  1.88 us (2%)
    pallas_call x1, Pallas kernels, fused(): pl.pallas_call(body, out_shape=jax.ShapeDtypeStruct((rows, out_cols), bf1...  74.9 us
    unnamed x1, local copies, waits for them, and re-layouts  1.88 us

profile of v3, /device:TPU:25, one launch (start us, length us, event | category | flops | bytes accessed | tf_op | source)
XLA Modules:
  0.0 77.3 jit_solution(17610295033020487528)
XLA Ops:
  0.0 0.5 multiply_power_fusion.refs_3_
  0.5 74.9 %fused.1 = bf16[128,2048]{1,0:T(8,128)(2,1)} custom-call(bf16[128,2048]{1,0:T(8,128)(2,1)} %refs_0_.1, f32[1,2048]{1,0:T(1,128)} %bitcast.2, f32[4,256]{1,0:T(4,128)} %bitcast.3, f32[1,128]{1,0:T(1,128)} %multiply_power_fusion.refs_3_, bf16[1024,128]{1,0:T(8,128)(2,1)} %refs_4_.1, bf16[512,128]{1,0:T(8,128)(2,1)} %refs_5_.1, bf16[2048,1024]{1,0:T(8,128)(2,1)} %refs_6_.1, ...), custom_call_target="tpu_custom_call" | custom-call | tf_op jit(solution)/shard_map/fused/pallas_call | solution.py:1704
  75.5 1.9 %copy.13 = bf16[128,2048]{1,0:T(8,128)(2,1)} copy(bf16[128,2048]{1,0:T(8,128)(2,1)} %fused.1) | data formatting | bytes 1048576

commit v4 on v3

--- a/solution.py
+++ b/solution.py
@@ -14,6 +14,7 @@
 BLOCK = 128
 MESH = pl.DeviceIdType.MESH
 VMEM_LIMIT = 60 * 1024 * 1024
+FUSED_LIMIT = 52 * 1024 * 1024
 
 eps = 1e-06
 
@@ -787,14 +788,16 @@
 def fused_kernel(
     n_sp,
     total,
-    tok_ref,
-    gain_ref,
-    gates_ref,
-    inv_ref,
+    tok_in,
+    gain_in,
+    gates_in,
     wr_ref,
     wf_ref,
     w_in,
     out,
+    tok_ref,
+    gain_ref,
+    gates_ref,
     xall,
     w_ret,
     w_fox,
@@ -901,6 +904,13 @@
         )
     pl.semaphore_signal(barrier, inc=1, device_id=(sp, other_core), device_id_type=MESH)
 
+    first = [
+        pltpu.make_async_copy(tok_in, tok_ref, local_sem.at[9]),
+        pltpu.make_async_copy(gain_in, gain_ref, local_sem.at[10]),
+        pltpu.make_async_copy(gates_in, gates_ref, local_sem.at[11]),
+    ]
+    for copy in first:
+        copy.start()
     locals_ = [
         pltpu.make_async_copy(wr_ref, wrs, local_sem.at[0]),
         pltpu.make_async_copy(
@@ -923,6 +933,8 @@
     for copy in locals_ + loads:
         copy.start()
 
+    for copy in first:
+        copy.wait()
     values = tok_ref[...].astype(f32)
     scale = lax.rsqrt(jnp.mean(values * values, axis=1, keepdims=True) + eps)
     xall[0, tp] = (values * scale * gain_ref[...]).astype(bf16)
@@ -1156,7 +1168,9 @@
         steps = offset.astype(f32)
         qdec[h] = jnp.exp(-rate * (steps + 1.0))
         kdec[h] = jnp.exp(-rate * (tok - 1.0 - steps))
-    inverse_freq = inv_ref[...]
+    half_head = RET_DIM // 2
+    index = lax.broadcasted_iota(jnp.int32, (1, half_head), 1).astype(f32)
+    inverse_freq = jnp.exp(index * (-math.log(10000.0) / half_head))
     unit = 16
     low = lax.broadcasted_iota(jnp.int32, (unit, RET_DIM // 2), 0).astype(f32)
     high = lax.broadcasted_iota(jnp.int32, (tok // unit, RET_DIM // 2), 0).astype(f32)
@@ -1167,8 +1181,6 @@
         ca, sa = cos_high[a : a + 1], sin_high[a : a + 1]
         ctab[a * unit : (a + 1) * unit] = cos_low * ca - sin_low * sa
         stab[a * unit : (a + 1) * unit] = sin_low * ca + cos_low * sa
-
-    half_head = RET_DIM // 2
 
     run_decay = [jnp.exp(-rates[h] * float(group * tok)) for h in range(hret)]
     tok_decay = [jnp.exp(-rates[h] * float(tok)) for h in range(hret)]
@@ -1241,11 +1253,18 @@
                 if i == 3:
                     sum_state()
             if m == 5:
-                ready = z < (last, 0, 1, 1)[i]
-
-                @pl.when(ready)
-                def _():
-                    kv_hop(z, i).start()
+                if i == 0:
+
+                    @pl.when(z < last)
+                    def _():
+                        kv_hop(z, 0).start()
+
+                elif i == 3:
+
+                    @pl.when(z == 0)
+                    def _():
+                        kv_hop(z, 2).start()
+                        kv_hop(z, 3).start()
 
             if m == 3 and i == 0:
                 for k in range(guests):
@@ -1593,6 +1612,7 @@
         phase("retain3", (retain, 3))
         phase("gates", (gate_columns,))
         phase("query0", (queries_of, 0))
+        phase("own_attention", (own_attention,))
         phase("up22", (line_up, 2, 2))
 
     @pl.when(z == last)
@@ -1610,13 +1630,13 @@
         phase("down22", (line_down, 2, 2))
         phase("retain3", (retain, 3))
         phase("gates", (gate_columns,))
+        phase("own_attention", (own_attention,))
         phase("plane_on", (plane_on,))
 
-    phase("own_attention", (own_attention,))
+    phase("retention_out", (retention_out,))
+    phase("late_pieces", (late_pieces,))
     for step in range(3, depth):
         phase("line2" + str(step), (line, 2, step))
-    phase("late_pieces", (late_pieces,))
-    phase("retention_out", (retention_out,))
     phase("ret_product1", (ret_product, 3, 1))
     phase("ret_product2", (ret_product, 2, 0))
     phase("serve0", (serve_first,))
@@ -1677,7 +1697,7 @@
     phase("settle", (settle_all,))
 
 
-def fused(tokens, gain, gates, inverse, w_ret, w_fox, w_in, hret, hfox, n_sp):
+def fused(tokens, gain, gates, w_ret, w_fox, w_in, hret, hfox, n_sp):
     rows, width = tokens.shape
     group = 4
     tok = 2 * rows
@@ -1687,7 +1707,7 @@
     ret_rows = hret * RET_DIM
     fox_rows = group * hfox * FOX_DIM
     vmem = pl.BlockSpec(memory_space=pltpu.VMEM)
-    hbm = pl.BlockSpec(memory_space=pl.ANY)
+    hbm = pl.BlockSpec(memory_space=pltpu.HBM)
     dma = pltpu.SemaphoreType.DMA
     f32 = jnp.float32
     bf16 = jnp.bfloat16
@@ -1698,15 +1718,18 @@
     total = float(tok * n_sp)
 
     def body(*refs):
-        fused_kernel(n_sp, total, *refs[:6], refs[6:12], *refs[12:])
+        fused_kernel(n_sp, total, *refs[:5], refs[5:11], *refs[11:])
 
     V = pltpu.VMEM
     return pl.pallas_call(
         body,
         out_shape=jax.ShapeDtypeStruct((rows, out_cols), bf16),
-        in_specs=[vmem] * 4 + [hbm] * 8,
+        in_specs=[hbm] * 11,
         out_specs=vmem,
         scratch_shapes=[
+            V(tokens.shape, bf16),
+            V(gain.shape, f32),
+            V(gates.shape, f32),
             V((group, 2, rows, width), bf16),
             V((3, width, ret_rows), bf16),
             V((3, width, hfox * FOX_DIM), bf16),
@@ -1749,7 +1772,7 @@
             V((tok, fox_rows), bf16),
             V((2, rows, out_cols), bf16),
             V((rows, out_cols), bf16),
-            dma((9,)),
+            dma((12,)),
             dma((3,)),
             dma((3,)),
             dma((3,)),
@@ -1782,10 +1805,15 @@
             dma((group,)),
         ],
         compiler_params=pltpu.CompilerParams(
-            collective_id=2, has_side_effects=True, vmem_limit_bytes=VMEM_LIMIT
+            collective_id=2, has_side_effects=True, vmem_limit_bytes=FUSED_LIMIT
         ),
         name="fused",
-    )(tokens, gain, gates, inverse, w_ret, w_fox, *w_in)
+    )(
+        *[
+            pltpu.with_memory_space_constraint(array, pltpu.HBM)
+            for array in (tokens, gain, gates, w_ret, w_fox, *w_in)
+        ]
+    )
 
 
 def decay_rates(head_ids, total):
@@ -1820,14 +1848,11 @@
     hret = ret_heads // group
     hfox = fox_heads // group
     run = rows * n_tp * group
-    half = RET_DIM // 2
-    inverse = 10000.0 ** (-jnp.arange(half, dtype=f32) / half)
     if group == 4 and n_tp == 2 and depth == 4:
         return fused(
             tokens,
             gain.reshape(1, width),
             fox_gates.T,
-            inverse.reshape(1, half),
             w_out_ret,
             w_out_fox,
             (w_ret_q, w_ret_k, w_ret_v, w_fox_q, w_fox_k, w_fox_v),
@@ -1840,6 +1865,8 @@
     z = sp // group
 
     positions = z * run + jnp.arange(run, dtype=jnp.int32)
+    half = RET_DIM // 2
+    inverse = 10000.0 ** (-jnp.arange(half, dtype=f32) / half)
     angles = positions.astype(f32)[:, None] * inverse[None, :]
     rq, rk, rv, fq, fkv, gall, wz = gather(
         tokens,

time: 77.8 us -> 73.8 us (0.949)
  Pallas kernels: 74.9 us -> 72.4 us
  local copies, waits for them, and re-layouts: 1.88 us -> 0.8 us
    pallas_call x1, Pallas kernels: 74.9 us -> 72.4 us  [fused(): pl.pallas_call(body, out_shape=jax.ShapeDtypeStruct((rows, out_cols), bf1...]
    unnamed x1, local copies, waits for them, and re-layouts: 1.88 us -> 0.8 us
where the time goes in v4:
time: 73.8 us; the launch traced here: 73.2 us
  Pallas kernels  72.4 us (98%)
  local copies, waits for them, and re-layouts  0.8 us (1%)
    pallas_call x1, Pallas kernels, fused(): pl.pallas_call(body, out_shape=jax.ShapeDtypeStruct((rows, out_cols), bf1...  72.4 us

profile of v4, /device:TPU:25, one launch (start us, length us, event | category | flops | bytes accessed | tf_op | source)
XLA Modules:
  0.0 73.2 jit_solution(2959988405686964271)
XLA Ops:
  0.0 72.4 %fused.1 = bf16[128,2048]{1,0:T(8,128)(2,1)S(1)} custom-call(bf16[128,2048]{1,0:T(8,128)(2,1)} %refs_0_.1, f32[1,2048]{1,0:T(1,128)} %bitcast.2, f32[4,256]{1,0:T(4,128)} %bitcast.3, bf16[1024,128]{1,0:T(8,128)(2,1)} %refs_3_.1, bf16[512,128]{1,0:T(8,128)(2,1)} %refs_4_.1, bf16[2048,1024]{1,0:T(8,128)(2,1)} %refs_5_.1, bf16[2048,1024]{1,0:T(8,128)(2,1)} %refs_6_.1, ...), custom_call_target="tpu_custom_call" | custom-call | tf_op jit(solution)/shard_map/fused/pallas_call | solution.py:1724
  72.4 0.8 %copy.13 = bf16[128,2048]{1,0:T(8,128)(2,1)} copy(bf16[128,2048]{1,0:T(8,128)(2,1)S(1)} %fused.1) | data formatting | bytes 1048576

commit v5 on v4

--- a/solution.py
+++ b/solution.py
@@ -1637,11 +1637,12 @@
     phase("late_pieces", (late_pieces,))
     for step in range(3, depth):
         phase("line2" + str(step), (line, 2, step))
-    phase("ret_product1", (ret_product, 3, 1))
-    phase("ret_product2", (ret_product, 2, 0))
+    phase("ret_product1", (ret_product, 3))
+    phase("ret_product2", (ret_product, 1, 2))
+    phase("scatter1a", (scatter_first, 3))
+    phase("ret_product3", (ret_product, 0))
     phase("serve0", (serve_first,))
-    phase("scatter1a", (scatter_first, 3, 1))
-    phase("scatter1b", (scatter_first, 2, 0))
+    phase("scatter1b", (scatter_first, 1, 2, 0))
     phase("serve1", (serve_rest,))
     phase("takes", (take_all,))
     phase("earlier", (earlier,))

time: 73.8 us -> 73.8 us (level)
  no operation moved by 1% of the time
where the time goes in v5:
time: 73.8 us; the launch traced here: 73 us
  Pallas kernels  72.1 us (98%)
  local copies, waits for them, and re-layouts  0.8 us (1%)
    pallas_call x1, Pallas kernels, fused(): pl.pallas_call(body, out_shape=jax.ShapeDtypeStruct((rows, out_cols), bf1...  72.1 us

profile of v5, /device:TPU:25, one launch (start us, length us, event | category | flops | bytes accessed | tf_op | source)
XLA Modules:
  0.0 73.0 jit_solution(9390656836052566638)
XLA Ops:
  0.0 72.1 %fused.1 = bf16[128,2048]{1,0:T(8,128)(2,1)S(1)} custom-call(bf16[128,2048]{1,0:T(8,128)(2,1)} %refs_0_.1, f32[1,2048]{1,0:T(1,128)} %bitcast.2, f32[4,256]{1,0:T(4,128)} %bitcast.3, bf16[1024,128]{1,0:T(8,128)(2,1)} %refs_3_.1, bf16[512,128]{1,0:T(8,128)(2,1)} %refs_4_.1, bf16[2048,1024]{1,0:T(8,128)(2,1)} %refs_5_.1, bf16[2048,1024]{1,0:T(8,128)(2,1)} %refs_6_.1, ...), custom_call_target="tpu_custom_call" | custom-call | tf_op jit(solution)/shard_map/fused/pallas_call | solution.py:1725
  72.2 0.8 %copy.13 = bf16[128,2048]{1,0:T(8,128)(2,1)} copy(bf16[128,2048]{1,0:T(8,128)(2,1)S(1)} %fused.1) | data formatting | bytes 1048576
